TPU v7x, 32 devices: a whole 2x2x4 slice. The times are simulated.
32 devices in a mesh: grp: 2 (over y), sp: 4 (over z), dp: 4 (over x, core).
Axes of the slice: x: 2, y: 2, z: 4, core: 2. Of those that a mesh axis runs over, the one named last changes fastest.
Arguments:
- query_rows: bfloat16 [8, 512, 2048], P(('grp', 'dp'), 'sp'), parts along dimension 0, may hold values from -6 to 6
- key_rows: bfloat16 [8, 512, 2048], P(('grp', 'dp'), 'sp'), parts along dimension 0, may hold values from -6 to 6
- value_rows: bfloat16 [8, 512, 2048], P(('grp', 'dp'), 'sp'), parts along dimension 0, may hold values from -6 to 6
- query_gain: float32 [64], replicated, may hold values from 1.1 to 7
- key_gain: float32 [64], replicated, may hold values from 1.1 to 7
- lambdas: float32 [16], replicated, may hold values from 0.3 to 0.8
- head_gain: float32 [128], replicated, may hold values from 0.1 to 1.9
- out_weight: bfloat16 [2048, 2048], P(None, 'dp'), may hold values from -0.125 to 0.125
Outputs:
- attended: bfloat16 [8, 512, 2048], P(('grp', 'dp'), 'sp'), parts along dimension 0
There are 2 independent parts, one for each index of `grp`. A program takes and returns all parts, laid end to end along the dimension named above; an argument that names none is the same for every part. Nothing has to cross between parts.
All inputs are finite; a program needn't handle non-finite values.
Results may differ from a plain program's by a relative error of at most 0.008.
The roundings to bfloat16 on the way count: a program that leaves them out, or rounds other values in their place, can miss the bound.
Values may be sent and summed in bfloat16 or wider, within the bound.
A program may use at most 128 MiB of HBM per device.

v0:
```python
import functools
import math

import jax
import jax.numpy as jnp
import numpy as np
from jax import lax
from jax.experimental import pallas as pl
from jax.experimental.pallas import tpu as pltpu
from jax.sharding import PartitionSpec as P

EPSILON = 1e-06
OUT_SCALE = 0.8
CORES = 2
CHUNKS = 2
WAYS = 2
MESH = pl.DeviceIdType.MESH


def rotation_tables(length, head_size):
    half = head_size // 2
    inverse = np.float32(10000.0) ** (-np.arange(half, dtype=np.float32) / np.float32(half))
    angles = np.arange(length, dtype=np.float32)[:, None] * inverse.astype(np.float32)[None, :]
    cosine, sine = np.cos(angles), np.sin(angles)
    return (
        np.concatenate([cosine] * 4, axis=1).astype(np.float32),
        np.concatenate([-sine, sine] * 2, axis=1).astype(np.float32),
    )


def kernel(
    n, n_dp, n_grp, head_size, q_ref, k_ref, v_ref, qg_ref, kg_ref, lam_ref, hg_ref, w_ref, cos_in, sin_in,
    out_ref, total, rx, rot_q, rot_k, heads_out, hrx, wfull,
    in_send, in_recv, ret_send, ret_recv, wx_send, wx_recv, wy_send, wy_recv, wc_send, wc_recv, own_sem, cos_ref, sin_ref, table_sem,
):
    me = lax.axis_index("sp")
    dp = lax.axis_index("dp")
    ways = WAYS if n_grp == WAYS else 1
    grp = lax.axis_index("grp") if ways > 1 else 0
    cores = CORES if n_dp % CORES == 0 else 1
    nx = n_dp // cores
    xi, core = dp // cores, lax.rem(dp, cores)
    tok = q_ref.shape[1]
    width = 2 * head_size
    local_heads = rx.shape[1]
    length = rx.shape[2]
    depth = w_ref.shape[0]
    cols = w_ref.shape[1]
    piece = depth // (CHUNKS * ways)

    def sp_peer(off):
        return lax.rem(me + off, n)

    def dp_index(xo, co):
        return lax.rem(xi + xo, nx) * cores + lax.rem(core + co, cores)

    barrier = pltpu.get_barrier_semaphore()
    for off in range(1, n):
        pl.semaphore_signal(barrier, inc=1, device_id={"sp": sp_peer(off)}, device_id_type=MESH)
    for xo in range(1, nx):
        pl.semaphore_signal(barrier, inc=1, device_id={"dp": dp_index(xo, 0)}, device_id_type=MESH)
    for co in range(1, cores):
        pl.semaphore_signal(barrier, inc=1, device_id={"dp": dp_index(0, co)}, device_id_type=MESH)

    if ways > 1:
        pl.semaphore_signal(
            barrier, inc=1, device_id={"grp": lax.rem(grp + 1, ways)}, device_id_type=MESH
        )

    sources = (k_ref, q_ref, v_ref)

    def own_rows(t, j):
        column = pl.multiple_of((me * local_heads + j) * width, width)
        return pltpu.make_async_copy(
            sources[t].at[0, :, pl.ds(column, width)],
            rx.at[t, j, pl.ds(pl.multiple_of(me * tok, tok), tok), :],
            in_recv.at[t, j, 0],
        )

    def rows_to(t, j, off):
        peer = sp_peer(off)
        column = pl.multiple_of((peer * local_heads + j) * width, width)
        return pltpu.make_async_remote_copy(
            src_ref=sources[t].at[0, :, pl.ds(column, width)],
            dst_ref=rx.at[t, j, pl.ds(pl.multiple_of(me * tok, tok), tok), :],
            send_sem=in_send.at[t, j, off],
            recv_sem=in_recv.at[t, j, off],
            device_id={"sp": peer},
            device_id_type=MESH,
        )

    def rows_from(t, j, off):
        peer = lax.rem(me + n - off, n)
        block = rx.at[t, j, pl.ds(pl.multiple_of(peer * tok, tok), tok), :]
        return pltpu.make_async_remote_copy(
            src_ref=block, dst_ref=block, send_sem=in_send.at[t, j, off],
            recv_sem=in_recv.at[t, j, off], device_id={"sp": peer}, device_id_type=MESH,
        )

    def piece_rows(r, way):
        first = (r * ways + lax.rem(grp + way, ways)) * piece
        return pl.ds(pl.multiple_of(first, piece), piece)

    def moved(source, target, send_sem, recv_sem, device):
        return pltpu.make_async_remote_copy(
            src_ref=source, dst_ref=target, send_sem=send_sem, recv_sem=recv_sem,
            device_id=device, device_id_type=MESH,
        )

    def weight_x(xo, r):
        rows = piece_rows(r, 0)
        return moved(
            w_ref.at[rows, :], wfull.at[dp, rows, :], wx_send.at[xo, r], wx_recv.at[xo, r],
            {"dp": dp_index(xo, 0)},
        )

    def weight_x_in(xo, r):
        block = wfull.at[dp_index(nx - xo, 0), piece_rows(r, 0), :]
        return moved(block, block, wx_send.at[xo, r], wx_recv.at[xo, r], {"dp": dp_index(xo, 0)})

    def weight_y(xo, r):
        block = wfull.at[dp_index(nx - xo, 0), piece_rows(r, 0), :]
        return moved(block, block, wy_send.at[xo, r], wy_recv.at[xo, r], {"grp": lax.rem(grp + 1, ways)})

    def weight_y_in(xo, r):
        block = wfull.at[dp_index(nx - xo, 0), piece_rows(r, 1), :]
        return moved(block, block, wy_send.at[xo, r], wy_recv.at[xo, r], {"grp": lax.rem(grp + 1, ways)})

    def weight_core(xo, r, way):
        rows = piece_rows(r, way)
        target = wfull.at[dp_index(nx - xo, 0), rows, :]
        return moved(
            w_ref.at[rows, :] if xo == 0 else target, target,
            wc_send.at[xo, r, way], wc_recv.at[xo, r, way], {"dp": dp_index(0, 1)},
        )

    def weight_core_in(xo, r, way):
        block = wfull.at[dp_index(nx - xo, 1), piece_rows(r, way), :]
        return moved(
            block, block, wc_send.at[xo, r, way], wc_recv.at[xo, r, way], {"dp": dp_index(0, 1)}
        )

    own_weight = pltpu.make_async_copy(w_ref, wfull.at[dp], own_sem)
    own_weight.start()
    tables = [
        pltpu.make_async_copy(cos_in, cos_ref, table_sem.at[0]),
        pltpu.make_async_copy(sin_in, sin_ref, table_sem.at[1]),
    ]
    for table in tables:
        table.start()
    for j in range(local_heads):
        for t in range(3):
            own_rows(t, j).start()
    pl.semaphore_wait(barrier, (n - 1) + (nx - 1) + (cores - 1) + (ways - 1))
    for j in range(local_heads):
        for t in range(3):
            for off in range(1, n):
                rows_to(t, j, off).start()
        if j == 0:
            for r in range(CHUNKS):
                for xo in range(1, nx):
                    weight_x(xo, r).start()
            if cores > 1:
                for r in range(CHUNKS):
                    for way in range(ways):
                        weight_core(0, r, way).start()

    lane = lax.broadcasted_iota(jnp.int32, (1, width), 1)
    low_map = lane < head_size
    low_half = lax.rem(lane, head_size) < head_size // 2

    def norm_rotate(block, gain):
        x = block.astype(jnp.float32)
        square = x * x
        low = jnp.sum(jnp.where(low_map, square, 0.0), axis=1, keepdims=True)
        high = jnp.sum(jnp.where(low_map, 0.0, square), axis=1, keepdims=True)
        low = lax.rsqrt(low * (1.0 / head_size) + EPSILON)
        high = lax.rsqrt(high * (1.0 / head_size) + EPSILON)
        y = x * jnp.where(low_map, low, high) * gain
        quarter = head_size // 2
        turned = jnp.where(low_half, pltpu.roll(y, width - quarter, 1), pltpu.roll(y, quarter, 1))
        return (y * cos_ref[...] + turned * sin_ref[...]).astype(jnp.bfloat16)

    def heads_to(j, i):
        column = pl.multiple_of(me * width, width)
        off = lax.rem(i + n - me, n)
        return pltpu.make_async_remote_copy(
            src_ref=heads_out.at[j, i], dst_ref=hrx.at[j, :, pl.ds(column, width)],
            send_sem=ret_send.at[j, off], recv_sem=ret_recv.at[j, off],
            device_id={"sp": i}, device_id_type=MESH,
        )

    def heads_from(j, off):
        peer = lax.rem(me + n - off, n)
        column = pl.multiple_of(peer * width, width)
        block = hrx.at[j, :, pl.ds(column, width)]
        return pltpu.make_async_remote_copy(
            src_ref=block, dst_ref=block, send_sem=ret_send.at[j, off],
            recv_sem=ret_recv.at[j, off], device_id={"sp": peer}, device_id_type=MESH,
        )

    groups = math.gcd(n, 4)
    per_group = n // groups
    segment = length // groups
    factor = head_size ** (-0.5) * math.log2(math.e)
    contract = (((1,), (1,)), ((), ()))

    def query_block(j, g, i, lam):
        rows = pl.ds(i * tok, tok) if isinstance(i, int) else pl.ds(pl.multiple_of(i * tok, tok), tok)
        q = rot_q[rows, :]
        zero = jnp.zeros_like(q)
        both = jnp.concatenate([jnp.where(low_map, q, zero), jnp.where(low_map, zero, q)], axis=0)
        start = g * segment
        spans = ([(0, start)] if g else []) + [(start, segment)]
        parts = []
        for first, size in spans:
            scores = lax.dot_general(
                both, rot_k[first : first + size, :], contract, preferred_element_type=jnp.float32
            )
            if first == start:
                shape = (2 * tok, size)
                row = lax.rem(lax.broadcasted_iota(jnp.int32, shape, 0), tok) + i * tok
                column = lax.broadcasted_iota(jnp.int32, shape, 1) + first
                scores = jnp.where(column <= row, scores, -1e30)
            parts.append(scores)
        top = functools.reduce(jnp.maximum, [jnp.max(s, axis=1, keepdims=True) for s in parts])
        parts = [jnp.exp2((s - top) * factor) for s in parts]
        total = functools.reduce(jnp.add, [jnp.sum(e, axis=1, keepdims=True) for e in parts])
        inverse = 1.0 / total
        one, two = inverse[:tok], inverse[tok:] * lam
        raw = None
        for (first, size), e in zip(spans, parts):
            mixing = (e[:tok] * one - e[tok:] * two).astype(jnp.bfloat16)
            term = jnp.dot(mixing, rx[2, j, first : first + size, :], preferred_element_type=jnp.float32)
            raw = term if raw is None else raw + term
        scaled = raw * lax.rsqrt(jnp.mean(raw * raw, axis=1, keepdims=True) + EPSILON)
        result = (scaled * hg_ref[...] * OUT_SCALE).astype(jnp.bfloat16)

        @pl.when(i == me)
        def _():
            hrx[j, :, pl.ds(pl.multiple_of(me * width, width), width)] = result

        @pl.when(i != me)
        def _():
            heads_out[j, i] = result
            heads_to(j, i).start()

    def forward(stage):
        if stage < CHUNKS:
            for xo in range(1, nx):
                weight_x_in(xo, stage).wait_recv()
                if ways > 1:
                    weight_y(xo, stage).start()
                if cores > 1:
                    weight_core(xo, stage, 0).start()
        elif ways > 1:
            for xo in range(1, nx):
                weight_y_in(xo, stage - CHUNKS).wait_recv()
                if cores > 1:
                    weight_core(xo, stage - CHUNKS, 1).start()

    for table in tables:
        table.wait()
    for j in range(local_heads):
        lam = lam_ref[me * local_heads + j]
        for t, (target, gain) in enumerate(((rot_k, kg_ref), (rot_q, qg_ref), (None, None))):
            own_rows(t, j).wait()
            for off in range(1, n):
                rows_from(t, j, off).wait_recv()
            if target is not None:
                target[...] = norm_rotate(rx[t, j], jnp.concatenate([gain[...]] * 2, axis=1))
        for g in range(groups):
            if per_group == 1:
                query_block(j, g, g, lam)
            else:
                def step(b, carry, j=j, g=g, lam=lam):
                    query_block(j, g, g * per_group + b, lam)
                    return carry
                lax.fori_loop(0, per_group, step, 0)
        for stage in range(2 * CHUNKS):
            if j == min(stage, local_heads - 1):
                forward(stage)

    own_weight.wait()
    if cores > 1:
        for xo in range(nx):
            for r in range(CHUNKS):
                for way in range(ways):
                    weight_core_in(xo, r, way).wait_recv()

    for j in range(local_heads):
        for off in range(1, n):
            heads_from(j, off).wait_recv()
        rows = hrx[j]
        for index in range(n_dp):
            matching = jnp.concatenate(
                [wfull[index, pl.ds((s * local_heads + j) * width, width), :] for s in range(n)], axis=0
            )
            term = jnp.dot(rows, matching, preferred_element_type=jnp.float32)
            span = slice(index * cols, (index + 1) * cols)
            if j:
                term = total[:, span] + term
            if j == local_heads - 1:
                out_ref[0, :, span] = term.astype(out_ref.dtype)
            else:
                total[:, span] = term

    for j in range(local_heads):
        for off in range(1, n):
            for t in range(3):
                rows_to(t, j, off).wait_send()
            heads_to(j, sp_peer(off)).wait_send()
    for r in range(CHUNKS):
        for xo in range(nx):
            if xo:
                weight_x(xo, r).wait_send()
                if ways > 1:
                    weight_y(xo, r).wait_send()
            if cores > 1:
                for way in range(ways):
                    weight_core(xo, r, way).wait_send()


def local(n, n_dp, n_grp, query_rows, key_rows, value_rows, query_gain, key_gain, lambdas, head_gain, out_weight):
    tok = query_rows.shape[1]
    head_size = query_gain.shape[0]
    width = head_gain.shape[0]
    local_heads = lambdas.shape[0] // n
    length = tok * n
    depth, cols = out_weight.shape
    cores = CORES if n_dp % CORES == 0 else 1
    nx = n_dp // cores
    cosine, sine = rotation_tables(length, head_size)
    anywhere = pl.BlockSpec(memory_space=pl.ANY)
    vmem = pl.BlockSpec(memory_space=pltpu.VMEM)
    dma = pltpu.SemaphoreType.DMA
    return pl.pallas_call(
        functools.partial(kernel, n, n_dp, n_grp, head_size),
        out_shape=jax.ShapeDtypeStruct((1, tok, n_dp * cols), jnp.bfloat16),
        in_specs=[anywhere] * 3
        + [vmem, vmem, pl.BlockSpec(memory_space=pltpu.SMEM), vmem, anywhere, anywhere, anywhere],
        out_specs=vmem,
        scratch_shapes=[
            pltpu.VMEM((tok, n_dp * cols), jnp.float32),
            pltpu.VMEM((3, local_heads, length, width), jnp.bfloat16),
            pltpu.VMEM((length, width), jnp.bfloat16),
            pltpu.VMEM((length, width), jnp.bfloat16),
            pltpu.VMEM((local_heads, n, tok, width), jnp.bfloat16),
            pltpu.VMEM((local_heads, tok, n * width), jnp.bfloat16),
            pltpu.VMEM((n_dp, depth, cols), jnp.bfloat16),
            dma((3, local_heads, n)),
            dma((3, local_heads, n)),
            dma((local_heads, n)),
            dma((local_heads, n)),
            dma((nx, CHUNKS)),
            dma((nx, CHUNKS)),
            dma((nx, CHUNKS)),
            dma((nx, CHUNKS)),
            dma((nx, CHUNKS, WAYS)),
            dma((nx, CHUNKS, WAYS)),
            dma(()),
            pltpu.VMEM((length, width), jnp.float32),
            pltpu.VMEM((length, width), jnp.float32),
            dma((2,)),
        ],
        compiler_params=pltpu.CompilerParams(
            collective_id=0, has_side_effects=True, vmem_limit_bytes=56 * 1024 * 1024
        ),
    )(
        query_rows, key_rows, value_rows,
        query_gain[None, :], key_gain[None, :], lambdas, head_gain[None, :],
        out_weight, jnp.asarray(cosine), jnp.asarray(sine),
    )


def solution(mesh):
    rows = P(("grp", "dp"), "sp", None)
    return jax.shard_map(
        functools.partial(local, mesh.shape["sp"], mesh.shape["dp"], mesh.shape["grp"]),
        mesh=mesh,
        in_specs=(rows, rows, rows, P(), P(), P(), P(), P(None, "dp")),
        out_specs=rows,
        check_vma=False,
    )
```

profile of v0, /device:TPU:0, one launch (start us, length us, event | category | flops | bytes accessed | tf_op | source)
XLA Modules:
  0.0 56.4 jit_solution(15447624880903575897)
XLA Ops:
  0.0 54.6 %shard_map.100 = bf16[1,128,2048]{2,1,0:T(8,128)(2,1)} custom-call(bf16[1,128,2048]{2,1,0:T(8,128)(2,1)} %q_ref.1, bf16[1,128,2048]{2,1,0:T(8,128)(2,1)} %k_ref.1, bf16[1,128,2048]{2,1,0:T(8,128)(2,1)} %v_ref.1, f32[1,64]{1,0:T(1,128)} %bitcast.3, f32[1,64]{1,0:T(1,128)} %bitcast.4, f32[16]{0:T(128)} %lam_ref.1, f32[1,128]{1,0:T(1,128)} %bitcast.5, ...), custom_call_target="tpu_custom_call" | custom-call | tf_op jit(solution)/shard_map/pallas_call | solution.py:337
  54.6 1.9 %copy.12 = bf16[1,128,2048]{2,1,0:T(8,128)(2,1)} copy(bf16[1,128,2048]{2,1,0:T(8,128)(2,1)} %shard_map.100) | data formatting | bytes 1048576
where the time goes:
time: 56.6 us; the launch traced here: 56.4 us
  Pallas kernels  54.6 us (96%)
  local copies, waits for them, and re-layouts  1.88 us (3%)
    pallas_call x1, Pallas kernels, local(): pl.pallas_call(functools.partial(kernel, n, n_dp, n_grp, head_size), out_...  54.6 us
    unnamed x1, local copies, waits for them, and re-layouts  1.88 us

commit v1 on v0

--- a/solution.py
+++ b/solution.py
@@ -14,6 +14,9 @@
 CORES = 2
 CHUNKS = 2
 WAYS = 2
+PARTS = 4
+GROUP = 4
+LAG = 3
 MESH = pl.DeviceIdType.MESH
 
 
@@ -373,10 +376,499 @@
     )
 
 
+def split_kernel(
+    n, n_dp, n_grp, head_size, chunks, q_in, k_in, v_in, qg_ref, kg_ref, lam_ref, hg_ref, w_ref, cos_in, sin_in,
+    out_ref, total, rows_in, q_rot, k_rot, v_turn, big, small, big_out, small_out, kept, kept_top, gain_turn, heads, wfull,
+    cos_ref, sin_ref, load_sem, big_send, big_recv, small_send, small_recv,
+    wx_send, wx_recv, wy_send, wy_recv, wc_send, wc_recv,
+):
+    me = lax.axis_index("sp")
+    dp = lax.axis_index("dp")
+    ways = WAYS if n_grp == WAYS else 1
+    grp = lax.axis_index("grp") if ways > 1 else 0
+    cores = CORES if n_dp % CORES == 0 else 1
+    nx = n_dp // cores
+    xi, core = dp // cores, lax.rem(dp, cores)
+    count, tok, width = q_rot.shape
+    depth, cols = w_ref.shape
+    piece = depth // (chunks * ways)
+    factor = head_size ** (-0.5) * math.log2(math.e)
+
+    def dp_index(xo, co):
+        return lax.rem(xi + xo, nx) * cores + lax.rem(core + co, cores)
+
+    barrier = pltpu.get_barrier_semaphore()
+    for off in range(1, n):
+        pl.semaphore_signal(barrier, inc=1, device_id={"sp": lax.rem(me + off, n)}, device_id_type=MESH)
+    for xo in range(1, nx):
+        pl.semaphore_signal(barrier, inc=1, device_id={"dp": dp_index(xo, 0)}, device_id_type=MESH)
+    for co in range(1, cores):
+        pl.semaphore_signal(barrier, inc=1, device_id={"dp": dp_index(0, co)}, device_id_type=MESH)
+    if ways > 1:
+        pl.semaphore_signal(barrier, inc=1, device_id={"grp": lax.rem(grp + 1, ways)}, device_id_type=MESH)
+
+    own = pl.ds(pl.multiple_of(me * tok, tok), tok)
+    loads = [
+        pltpu.make_async_copy(q_in.at[0], rows_in.at[0], load_sem.at[0]),
+        pltpu.make_async_copy(k_in.at[0], rows_in.at[1], load_sem.at[1]),
+        pltpu.make_async_copy(v_in.at[0], rows_in.at[2], load_sem.at[2]),
+        pltpu.make_async_copy(cos_in.at[own, :], cos_ref, load_sem.at[3]),
+        pltpu.make_async_copy(sin_in.at[own, :], sin_ref, load_sem.at[4]),
+    ]
+    own_weight = pltpu.make_async_copy(w_ref, wfull.at[dp], load_sem.at[5])
+    for load in loads:
+        load.start()
+    own_weight.start()
+
+    def moved(source, target, send_sem, recv_sem, device):
+        return pltpu.make_async_remote_copy(
+            src_ref=source, dst_ref=target, send_sem=send_sem, recv_sem=recv_sem,
+            device_id=device, device_id_type=MESH,
+        )
+
+    def piece_rows(r, way):
+        first = (r * ways + lax.rem(grp + way, ways)) * piece
+        return pl.ds(pl.multiple_of(first, piece), piece)
+
+    def weight_x(xo, r):
+        rows = piece_rows(r, 0)
+        return moved(
+            w_ref.at[rows, :], wfull.at[dp, rows, :], wx_send.at[xo, r], wx_recv.at[xo, r],
+            {"dp": dp_index(xo, 0)},
+        )
+
+    def weight_x_in(xo, r):
+        block = wfull.at[dp_index(nx - xo, 0), piece_rows(r, 0), :]
+        return moved(block, block, wx_send.at[xo, r], wx_recv.at[xo, r], {"dp": dp_index(xo, 0)})
+
+    def weight_y(xo, r):
+        block = wfull.at[dp_index(nx - xo, 0), piece_rows(r, 0), :]
+        return moved(block, block, wy_send.at[xo, r], wy_recv.at[xo, r], {"grp": lax.rem(grp + 1, ways)})
+
+    def weight_y_in(xo, r):
+        block = wfull.at[dp_index(nx - xo, 0), piece_rows(r, 1), :]
+        return moved(block, block, wy_send.at[xo, r], wy_recv.at[xo, r], {"grp": lax.rem(grp + 1, ways)})
+
+    def weight_core(xo, r, way):
+        rows = piece_rows(r, way)
+        target = wfull.at[dp_index(nx - xo, 0), rows, :]
+        return moved(
+            w_ref.at[rows, :] if xo == 0 else target, target,
+            wc_send.at[xo, r, way], wc_recv.at[xo, r, way], {"dp": dp_index(0, 1)},
+        )
+
+    def weight_core_in(xo, r, way):
+        block = wfull.at[dp_index(nx - xo, 1), piece_rows(r, way), :]
+        return moved(block, block, wc_send.at[xo, r, way], wc_recv.at[xo, r, way], {"dp": dp_index(0, 1)})
+
+    def forward_x(r):
+        for xo in range(1, nx):
+            weight_x_in(xo, r).wait_recv()
+            if ways > 1:
+                weight_y(xo, r).start()
+            if cores > 1:
+                weight_core(xo, r, 0).start()
+
+    def forward_y(r):
+        if ways > 1:
+            for xo in range(1, nx):
+                weight_y_in(xo, r).wait_recv()
+                if cores > 1:
+                    weight_core(xo, r, 1).start()
+
+    def big_to(source, lane, slot, h, peer):
+        return moved(source.at[h], big.at[slot, h], big_send.at[lane, h], big_recv.at[slot, h], {"sp": peer})
+
+    def small_to(lane, slot, h, peer):
+        return moved(
+            small_out.at[lane, h], small.at[slot, h], small_send.at[lane, h], small_recv.at[slot, h], {"sp": peer}
+        )
+
+    def big_in(slot, h):
+        block = big.at[slot, h]
+        moved(block, block, big_send.at[0, h], big_recv.at[slot, h], {"sp": lax.rem(me + 1, n)}).wait_recv()
+
+    def small_in(slot, h):
+        block = small.at[slot, h]
+        moved(block, block, small_send.at[0, h], small_recv.at[slot, h], {"sp": lax.rem(me + 1, n)}).wait_recv()
+
+    pl.semaphore_wait(barrier, (n - 1) + (nx - 1) + (cores - 1) + (ways - 1))
+    for r in range(chunks):
+        for xo in range(1, nx):
+            weight_x(xo, r).start()
+    if cores > 1:
+        for r in range(chunks):
+            for way in range(ways):
+                weight_core(0, r, way).start()
+
+    lane = lax.broadcasted_iota(jnp.int32, (1, width), 1)
+    low_map = lane < head_size
+    low_half = lax.rem(lane, head_size) < head_size // 2
+
+    def norm_rotate(block, gain):
+        x = block.astype(jnp.float32)
+        square = x * x
+        low = jnp.sum(jnp.where(low_map, square, 0.0), axis=1, keepdims=True)
+        high = jnp.sum(jnp.where(low_map, 0.0, square), axis=1, keepdims=True)
+        low = lax.rsqrt(low * (1.0 / head_size) + EPSILON)
+        high = lax.rsqrt(high * (1.0 / head_size) + EPSILON)
+        y = x * jnp.where(low_map, low, high) * gain
+        quarter = head_size // 2
+        turned = jnp.where(low_half, pltpu.roll(y, width - quarter, 1), pltpu.roll(y, quarter, 1))
+        return (y * cos_ref[...] + turned * sin_ref[...]).astype(jnp.bfloat16)
+
+    for load in loads:
+        load.wait()
+    gain_turn[...] = jnp.broadcast_to(hg_ref[...], (tok, width)).T
+    q_gain = jnp.concatenate([qg_ref[...]] * 2, axis=1)
+    k_gain = jnp.concatenate([kg_ref[...]] * 2, axis=1)
+    causal = lax.broadcasted_iota(jnp.int32, (tok, 2 * tok), 0) <= lax.rem(
+        lax.broadcasted_iota(jnp.int32, (tok, 2 * tok), 1), tok
+    )
+
+    def head_columns(h):
+        return pl.ds(pl.multiple_of(h * width, width), width)
+
+    def turned_scores(keys, q):
+        zero = jnp.zeros_like(q)
+        both = jnp.concatenate([jnp.where(low_map, q, zero), jnp.where(low_map, zero, q)], axis=0)
+        return lax.dot_general(keys, both, (((1,), (1,)), ((), ())), preferred_element_type=jnp.float32)
+
+    def exponents(scores):
+        top = jnp.max(scores, axis=0, keepdims=True)
+        e = jnp.exp2((scores - top) * factor)
+        return top * factor, e, jnp.sum(e, axis=0, keepdims=True)
+
+    def mixed(e, scale, lam, values):
+        one, two = scale[:, :tok], scale[:, tok:] * lam
+        mixing = (e[:, :tok] * one - e[:, tok:] * two).astype(jnp.bfloat16)
+        return jnp.dot(values, mixing, preferred_element_type=jnp.float32)
+
+    def put_pair(ref, first, h, pair):
+        ref[first, h, 0:1, :] = pair[:, :tok]
+        ref[first, h, 1:2, :] = pair[:, tok:]
+
+    def get_pair(ref, first, h):
+        return jnp.concatenate([ref[first, h, 0:1, :], ref[first, h, 1:2, :]], axis=1)
+
+    def joined(levels):
+        top = functools.reduce(jnp.maximum, levels)
+        return top + jnp.log2(functools.reduce(jnp.add, [jnp.exp2(l - top) for l in levels]))
+
+    def finish(raw, h):
+        scaled = raw * lax.rsqrt(jnp.mean(raw * raw, axis=0, keepdims=True) + EPSILON)
+        result = (scaled * gain_turn[...] * OUT_SCALE).T
+        heads[:, head_columns(h)] = result.astype(jnp.bfloat16)
+
+    def partial_scores(keys, q, slot, h, masked):
+        scores = turned_scores(keys, q)
+        if masked:
+            scores = jnp.where(causal, scores, -1e30)
+        top, e, z = exponents(scores)
+        kept[slot, h] = e
+        put_pair(kept_top, slot, h, top)
+        put_pair(small_out, slot, h, top + jnp.log2(z))
+
+    def prepare(h, carry):
+        span = head_columns(h)
+        q_rot[h] = norm_rotate(rows_in[0, :, span], q_gain)
+
+        @pl.when(me == 2)
+        def _():
+            big_to(q_rot, 0, 2, h, 1).start()
+
+        @pl.when(me == 3)
+        def _():
+            big_to(q_rot, 1, 3, h, 2).start()
+            big_to(q_rot, 0, 3, h, 1).start()
+
+        k_rot[h] = norm_rotate(rows_in[1, :, span], k_gain)
+        v_turn[h] = rows_in[2, :, span].astype(jnp.float32).T.astype(jnp.bfloat16)
+
+        @pl.when(me == 0)
+        def _():
+            big_to(k_rot, 0, 0, h, 1).start()
+            big_to(v_turn, 1, 1, h, 1).start()
+
+        @pl.when(me >= 2)
+        def _():
+            partial_scores(k_rot[h], q_rot[h], 0, h, True)
+            small_to(0, me - 2, h, 1).start()
+
+        return carry
+
+    lax.fori_loop(0, count, prepare, 0)
+
+    def lowest(h):
+        scores = jnp.where(causal, turned_scores(k_rot[h], q_rot[h]), -1e30)
+        _, e, z = exponents(scores)
+        finish(mixed(e, 1.0 / z, lam_ref[h], v_turn[h]), h)
+
+    def centre_keys(h):
+        return (
+            jnp.concatenate([big[0, h], k_rot[h]], axis=0),
+            jnp.concatenate([big[1, h], v_turn[h]], axis=1),
+        )
+
+    def served(h, slot, levels, keys, values):
+        top, e, z = exponents(turned_scores(keys, big[slot, h]))
+        level = joined([top + jnp.log2(z)] + levels)
+        big_out[slot - 2, h] = mixed(e, jnp.exp2(top - level), lam_ref[h], values).astype(jnp.bfloat16)
+        put_pair(small_out, slot - 2, h, level)
+
+    def centre_second(h):
+        big_in(0, h)
+        big_in(1, h)
+        big_in(2, h)
+        small_in(0, h)
+        keys, values = centre_keys(h)
+        served(h, 2, [get_pair(small, 0, h)], keys, values)
+        scores = turned_scores(keys, q_rot[h])
+        scores = jnp.concatenate([scores[:tok], jnp.where(causal, scores[tok:], -1e30)], axis=0)
+        _, e, z = exponents(scores)
+        finish(mixed(e, 1.0 / z, lam_ref[h], values), h)
+        big_to(big_out.at[0], 0, 0, h, 2).start()
+        small_to(0, 0, h, 2).start()
+
+    def centre_third(h):
+        big_in(3, h)
+        small_in(1, h)
+        small_in(2, h)
+        keys, values = centre_keys(h)
+        served(h, 3, [get_pair(small, 1, h), get_pair(small, 2, h)], keys, values)
+        small_to(1, 1, h, 2).start()
+        big_to(big_out.at[1], 1, 0, h, 3).start()
+        moved(
+            small_out.at[1, h], small.at[1, h], small_send.at[2, h], small_recv.at[1, h], {"sp": 3}
+        ).start()
+
+    def upper_scores(h):
+        big_in(3, h)
+        partial_scores(k_rot[h], big[3, h], 1, h, False)
+        small_to(1, 2, h, 1).start()
+
+    def upper_raw(h, slot, level):
+        scale = jnp.exp2(get_pair(kept_top, slot, h) - level)
+        return mixed(kept[slot, h], scale, lam_ref[h], v_turn[h])
+
+    def upper_help(h):
+        small_in(1, h)
+        big_out[1, h] = upper_raw(h, 1, get_pair(small, 1, h)).astype(jnp.bfloat16)
+        big_to(big_out.at[1], 1, 1, h, 3).start()
+
+    def upper_second(h):
+        big_in(0, h)
+        small_in(0, h)
+        finish(upper_raw(h, 0, get_pair(small, 0, h)) + big[0, h].astype(jnp.float32), h)
+
+    def upper_third(h):
+        big_in(0, h)
+        small_in(1, h)
+        big_in(1, h)
+        raw = upper_raw(h, 0, get_pair(small, 1, h)) + big[0, h].astype(jnp.float32)
+        finish(raw + big[1, h].astype(jnp.float32), h)
+
+    group = GROUP
+    per_chunk = count // chunks
+
+    def project(g, first, last):
+        step = group * width
+        rows = pl.ds(g * step, step) if isinstance(g, int) else pl.ds(pl.multiple_of(g * step, step), step)
+        if cores > 1:
+            for xo in range(nx):
+                for r in range(group // per_chunk):
+                    for way in range(ways):
+                        weight_core_in(xo, g * (group // per_chunk) + r, way).wait_recv()
+        block = heads[:, rows]
+        for index in range(n_dp):
+            term = jnp.dot(block, wfull[index, rows, :], preferred_element_type=jnp.float32)
+            span = slice(index * cols, (index + 1) * cols)
+            if not first:
+                term = total[:, span] + term
+            if last:
+                out_ref[0, :, span] = term.astype(out_ref.dtype)
+            else:
+                total[:, span] = term
+
+    groups = count // group
+    late = 2 * group + 1
+
+    def step(it, carry):
+        @pl.when((me == 0) & (it < count))
+        def _():
+            lowest(it)
+
+        @pl.when((me == 1) & (it < count))
+        def _():
+            centre_second(it)
+
+        @pl.when((me == 1) & (it >= 1) & (it <= count))
+        def _():
+            centre_third(it - 1)
+
+        @pl.when((me == 2) & (it < count))
+        def _():
+            upper_scores(it)
+
+        @pl.when((me == 2) & (it >= LAG))
+        def _():
+            upper_help(it - LAG)
+            upper_second(it - LAG)
+
+        @pl.when((me == 3) & (it >= LAG))
+        def _():
+            upper_third(it - LAG)
+
+        turn = lax.rem(it, per_chunk) == 0
+
+        @pl.when(turn & (it >= per_chunk) & (it <= count))
+        def _():
+            forward_x(it // per_chunk - 1)
+
+        first_y = 3 * per_chunk
+
+        @pl.when(turn & (it >= first_y))
+        def _():
+            forward_y((it - first_y) // per_chunk)
+
+        for g in range(groups - 1):
+            @pl.when(it == g * group + late)
+            def _(g=g):
+                if g == 0:
+                    own_weight.wait()
+                project(g, g == 0, False)
+
+        return carry
+
+    steps = count + LAG
+    lax.fori_loop(0, steps, step, 0)
+    for r in range((steps - 1 - 3 * per_chunk) // per_chunk + 1, chunks):
+        forward_y(r)
+    project(groups - 1, False, True)
+
+    def drain(h, carry):
+        @pl.when(me == 0)
+        def _():
+            big_to(k_rot, 0, 0, h, 1).wait_send()
+            big_to(v_turn, 1, 1, h, 1).wait_send()
+
+        @pl.when(me == 1)
+        def _():
+            big_to(big_out.at[0], 0, 0, h, 2).wait_send()
+            small_to(0, 0, h, 2).wait_send()
+            small_to(1, 1, h, 2).wait_send()
+            big_to(big_out.at[1], 1, 0, h, 3).wait_send()
+            moved(
+                small_out.at[1, h], small.at[1, h], small_send.at[2, h], small_recv.at[1, h], {"sp": 3}
+            ).wait_send()
+
+        @pl.when(me == 2)
+        def _():
+            big_to(q_rot, 0, 2, h, 1).wait_send()
+            small_to(0, 0, h, 1).wait_send()
+            small_to(1, 2, h, 1).wait_send()
+            big_to(big_out.at[1], 1, 1, h, 3).wait_send()
+
+        @pl.when(me == 3)
+        def _():
+            big_to(q_rot, 1, 3, h, 2).wait_send()
+            big_to(q_rot, 0, 3, h, 1).wait_send()
+            small_to(0, 1, h, 1).wait_send()
+
+        return carry
+
+    lax.fori_loop(0, count, drain, 0)
+
+    def drain_weights(r, carry):
+        for xo in range(nx):
+            if xo:
+                weight_x(xo, r).wait_send()
+                if ways > 1:
+                    weight_y(xo, r).wait_send()
+            if cores > 1:
+                for way in range(ways):
+                    weight_core(xo, r, way).wait_send()
+        return carry
+
+    lax.fori_loop(0, chunks, drain_weights, 0)
+
+
+def split_local(n, n_dp, n_grp, query_rows, key_rows, value_rows, query_gain, key_gain, lambdas, head_gain, out_weight):
+    tok = query_rows.shape[1]
+    head_size = query_gain.shape[0]
+    width = head_gain.shape[0]
+    count = lambdas.shape[0]
+    depth, cols = out_weight.shape
+    ways = WAYS if n_grp == WAYS else 1
+    chunks = count // ways
+    cores = CORES if n_dp % CORES == 0 else 1
+    nx = n_dp // cores
+    cosine, sine = rotation_tables(tok * n, head_size)
+    anywhere = pl.BlockSpec(memory_space=pl.ANY)
+    vmem = pl.BlockSpec(memory_space=pltpu.VMEM)
+    dma = pltpu.SemaphoreType.DMA
+    block = (count, tok, width)
+    return pl.pallas_call(
+        functools.partial(split_kernel, n, n_dp, n_grp, head_size, chunks),
+        out_shape=jax.ShapeDtypeStruct((1, tok, n_dp * cols), jnp.bfloat16),
+        in_specs=[anywhere] * 3
+        + [vmem, vmem, pl.BlockSpec(memory_space=pltpu.SMEM), vmem, anywhere, anywhere, anywhere],
+        out_specs=vmem,
+        scratch_shapes=[
+            pltpu.VMEM((tok, n_dp * cols), jnp.float32),
+            pltpu.VMEM((3, tok, count * width), jnp.bfloat16),
+            pltpu.VMEM(block, jnp.bfloat16),
+            pltpu.VMEM(block, jnp.bfloat16),
+            pltpu.VMEM(block, jnp.bfloat16),
+            pltpu.VMEM((4,) + block, jnp.bfloat16),
+            pltpu.VMEM((3, count, 2, tok), jnp.float32),
+            pltpu.VMEM((2,) + block, jnp.bfloat16),
+            pltpu.VMEM((2, count, 2, tok), jnp.float32),
+            pltpu.VMEM((2, count, tok, 2 * tok), jnp.float32),
+            pltpu.VMEM((2, count, 2, tok), jnp.float32),
+            pltpu.VMEM((width, tok), jnp.float32),
+            pltpu.VMEM((tok, count * width), jnp.bfloat16),
+            pltpu.VMEM((n_dp, depth, cols), jnp.bfloat16),
+            pltpu.VMEM((tok, width), jnp.float32),
+            pltpu.VMEM((tok, width), jnp.float32),
+            dma((6,)),
+            dma((2, count)),
+            dma((4, count)),
+            dma((3, count)),
+            dma((3, count)),
+            dma((nx, chunks)),
+            dma((nx, chunks)),
+            dma((nx, chunks)),
+            dma((nx, chunks)),
+            dma((nx, chunks, ways)),
+            dma((nx, chunks, ways)),
+        ],
+        compiler_params=pltpu.CompilerParams(
+            collective_id=0, has_side_effects=True, vmem_limit_bytes=56 * 1024 * 1024
+        ),
+    )(
+        query_rows, key_rows, value_rows,
+        query_gain[None, :], key_gain[None, :], lambdas, head_gain[None, :],
+        out_weight, jnp.asarray(cosine), jnp.asarray(sine),
+    )
+
+
+def plan(n, tok, width, count, n_grp):
+    ways = WAYS if n_grp == WAYS else 1
+    fits = n == PARTS and tok == width and count % (GROUP * ways) == 0
+    return split_local if fits else local
+
+
 def solution(mesh):
     rows = P(("grp", "dp"), "sp", None)
+    n, n_dp, n_grp = mesh.shape["sp"], mesh.shape["dp"], mesh.shape["grp"]
+
+    def body(*args):
+        chosen = plan(n, args[0].shape[1], args[6].shape[0], args[5].shape[0], n_grp)
+        return chosen(n, n_dp, n_grp, *args)
+
     return jax.shard_map(
-        functools.partial(local, mesh.shape["sp"], mesh.shape["dp"], mesh.shape["grp"]),
+        body,
         mesh=mesh,
         in_specs=(rows, rows, rows, P(), P(), P(), P(), P(None, "dp")),
         out_specs=rows,

time: 56.6 us -> 68.4 us (1.21)
  the two profiles are of different devices: /device:TPU:0 before, /device:TPU:27 now
where the time goes in v1:
time: 68.4 us; the launch traced here: 68.2 us
  Pallas kernels  66.3 us (97%)
  local copies, waits for them, and re-layouts  1.88 us (3%)
    pallas_call x1, Pallas kernels, split_local(): pl.pallas_call(functools.partial(split_kernel, n, n_dp, n_grp, head_size,...  66.3 us
    unnamed x1, local copies, waits for them, and re-layouts  1.88 us

profile of v1, /device:TPU:27, one launch (start us, length us, event | category | flops | bytes accessed | tf_op | source)
XLA Modules:
  0.0 68.2 jit_solution(8972862334168659633)
XLA Ops:
  0.0 66.3 %shard_map.100 = bf16[1,128,2048]{2,1,0:T(8,128)(2,1)} custom-call(bf16[1,128,2048]{2,1,0:T(8,128)(2,1)} %q_in.1, bf16[1,128,2048]{2,1,0:T(8,128)(2,1)} %k_in.1, bf16[1,128,2048]{2,1,0:T(8,128)(2,1)} %v_in.1, f32[1,64]{1,0:T(1,128)} %bitcast.3, f32[1,64]{1,0:T(1,128)} %bitcast.4, f32[16]{0:T(128)} %lam_ref.1, f32[1,128]{1,0:T(1,128)} %bitcast.5, ...), custom_call_target="tpu_custom_call" | custom-call | tf_op jit(solution)/shard_map/pallas_call | solution.py:811
  66.3 1.9 %copy.12 = bf16[1,128,2048]{2,1,0:T(8,128)(2,1)} copy(bf16[1,128,2048]{2,1,0:T(8,128)(2,1)} %shard_map.100) | data formatting | bytes 1048576

commit v2 on v1

--- a/solution.py
+++ b/solution.py
@@ -16,7 +16,8 @@
 WAYS = 2
 PARTS = 4
 GROUP = 4
-LAG = 3
+LAG = 5
+AHEAD = 2
 MESH = pl.DeviceIdType.MESH
 
 
@@ -379,7 +380,7 @@
 def split_kernel(
     n, n_dp, n_grp, head_size, chunks, q_in, k_in, v_in, qg_ref, kg_ref, lam_ref, hg_ref, w_ref, cos_in, sin_in,
     out_ref, total, rows_in, q_rot, k_rot, v_turn, big, small, big_out, small_out, kept, kept_top, gain_turn, heads, wfull,
-    cos_ref, sin_ref, load_sem, big_send, big_recv, small_send, small_recv,
+    cos_ref, sin_ref, turn_ref, out_rows, load_sem, out_sem, big_send, big_recv, small_send, small_recv,
     wx_send, wx_recv, wy_send, wy_recv, wc_send, wc_recv,
 ):
     me = lax.axis_index("sp")
@@ -503,25 +504,37 @@
 
     lane = lax.broadcasted_iota(jnp.int32, (1, width), 1)
     low_map = lane < head_size
-    low_half = lax.rem(lane, head_size) < head_size // 2
-
-    def norm_rotate(block, gain):
-        x = block.astype(jnp.float32)
+    half = head_size // 2
+    down, across = (lax.broadcasted_iota(jnp.int32, (width, width), axis) for axis in range(2))
+    partner = jnp.where(lax.rem(across, head_size) < half, across + half, across - half)
+    swap = jnp.where(down == partner, 1.0, 0.0).astype(jnp.bfloat16)
+    same_map = jnp.where((down < head_size) == (across < head_size), 1.0, 0.0).astype(jnp.bfloat16)
+    sums = jnp.concatenate([same_map, same_map], axis=0)
+
+    def norm_rotate(which, target, first):
+        blocks = [rows_in[which, :, head_columns(first + i)] for i in range(GROUP)]
+        stacked = jnp.concatenate(blocks, axis=0)
+        x = stacked.astype(jnp.float32)
         square = x * x
-        low = jnp.sum(jnp.where(low_map, square, 0.0), axis=1, keepdims=True)
-        high = jnp.sum(jnp.where(low_map, 0.0, square), axis=1, keepdims=True)
-        low = lax.rsqrt(low * (1.0 / head_size) + EPSILON)
-        high = lax.rsqrt(high * (1.0 / head_size) + EPSILON)
-        y = x * jnp.where(low_map, low, high) * gain
-        quarter = head_size // 2
-        turned = jnp.where(low_half, pltpu.roll(y, width - quarter, 1), pltpu.roll(y, quarter, 1))
-        return (y * cos_ref[...] + turned * sin_ref[...]).astype(jnp.bfloat16)
+        coarse = square.astype(jnp.bfloat16)
+        fine = (square - coarse.astype(jnp.float32)).astype(jnp.bfloat16)
+        total_square = jnp.dot(jnp.concatenate([coarse, fine], axis=1), sums, preferred_element_type=jnp.float32)
+        other = jnp.dot(stacked, swap, preferred_element_type=jnp.float32)
+        inverse = lax.rsqrt(total_square * (1.0 / head_size) + EPSILON)
+        for i in range(GROUP):
+            part = slice(i * tok, (i + 1) * tok)
+            straight = x[part] * inverse[part] * turn_ref[2 * which]
+            turned = other[part] * inverse[part] * turn_ref[2 * which + 1]
+            target[first + i] = (straight + turned).astype(jnp.bfloat16)
 
     for load in loads:
         load.wait()
     gain_turn[...] = jnp.broadcast_to(hg_ref[...], (tok, width)).T
-    q_gain = jnp.concatenate([qg_ref[...]] * 2, axis=1)
-    k_gain = jnp.concatenate([kg_ref[...]] * 2, axis=1)
+    for which, gain in enumerate((qg_ref, kg_ref)):
+        gain = gain[...]
+        crossed = jnp.concatenate([gain[:, half:], gain[:, :half]], axis=1)
+        turn_ref[2 * which] = cos_ref[...] * jnp.concatenate([gain, gain], axis=1)
+        turn_ref[2 * which + 1] = sin_ref[...] * jnp.concatenate([crossed, crossed], axis=1)
     causal = lax.broadcasted_iota(jnp.int32, (tok, 2 * tok), 0) <= lax.rem(
         lax.broadcasted_iota(jnp.int32, (tok, 2 * tok), 1), tok
     )
@@ -529,9 +542,12 @@
     def head_columns(h):
         return pl.ds(pl.multiple_of(h * width, width), width)
 
-    def turned_scores(keys, q):
-        zero = jnp.zeros_like(q)
-        both = jnp.concatenate([jnp.where(low_map, q, zero), jnp.where(low_map, zero, q)], axis=0)
+    def turned_scores(keys, *queries):
+        both = []
+        for q in queries:
+            zero = jnp.zeros_like(q)
+            both += [jnp.where(low_map, q, zero), jnp.where(low_map, zero, q)]
+        both = jnp.concatenate(both, axis=0)
         return lax.dot_general(keys, both, (((1,), (1,)), ((), ())), preferred_element_type=jnp.float32)
 
     def exponents(scores):
@@ -539,10 +555,12 @@
         e = jnp.exp2((scores - top) * factor)
         return top * factor, e, jnp.sum(e, axis=0, keepdims=True)
 
+    def mixing_of(e, scale, lam):
+        one, two = scale[:, :tok], scale[:, tok:] * lam
+        return (e[:, :tok] * one - e[:, tok:] * two).astype(jnp.bfloat16)
+
     def mixed(e, scale, lam, values):
-        one, two = scale[:, :tok], scale[:, tok:] * lam
-        mixing = (e[:, :tok] * one - e[:, tok:] * two).astype(jnp.bfloat16)
-        return jnp.dot(values, mixing, preferred_element_type=jnp.float32)
+        return jnp.dot(values, mixing_of(e, scale, lam), preferred_element_type=jnp.float32)
 
     def put_pair(ref, first, h, pair):
         ref[first, h, 0:1, :] = pair[:, :tok]
@@ -560,92 +578,107 @@
         result = (scaled * gain_turn[...] * OUT_SCALE).T
         heads[:, head_columns(h)] = result.astype(jnp.bfloat16)
 
-    def partial_scores(keys, q, slot, h, masked):
-        scores = turned_scores(keys, q)
+    def partial_scores(keys, queries, slot, first, masked):
+        scores = [turned_scores(k, q) for k, q in zip(keys, queries)]
         if masked:
-            scores = jnp.where(causal, scores, -1e30)
-        top, e, z = exponents(scores)
-        kept[slot, h] = e
-        put_pair(kept_top, slot, h, top)
-        put_pair(small_out, slot, h, top + jnp.log2(z))
-
-    def prepare(h, carry):
-        span = head_columns(h)
-        q_rot[h] = norm_rotate(rows_in[0, :, span], q_gain)
-
-        @pl.when(me == 2)
-        def _():
-            big_to(q_rot, 0, 2, h, 1).start()
+            scores = [jnp.where(causal, s, -1e30) for s in scores]
+        parts = [exponents(s) for s in scores]
+        for i, (top, e, z) in enumerate(parts):
+            kept[slot, first + i] = e
+            put_pair(kept_top, slot, first + i, top)
+            put_pair(small_out, slot, first + i, top + jnp.log2(z))
+
+    def prepare(j, carry):
+        first = j * GROUP
+        norm_rotate(0, q_rot, first)
 
         @pl.when(me == 3)
         def _():
-            big_to(q_rot, 1, 3, h, 2).start()
-            big_to(q_rot, 0, 3, h, 1).start()
-
-        k_rot[h] = norm_rotate(rows_in[1, :, span], k_gain)
-        v_turn[h] = rows_in[2, :, span].astype(jnp.float32).T.astype(jnp.bfloat16)
+            for i in range(GROUP):
+                big_to(q_rot, 1, 3, first + i, 2).start()
+                big_to(q_rot, 0, 3, first + i, 1).start()
+
+        @pl.when((me == 2) & (j == 0))
+        def _():
+            for i in range(AHEAD):
+                big_to(q_rot, 0, 2, i, 1).start()
+
+        norm_rotate(1, k_rot, first)
+        for i in range(GROUP):
+            v_turn[first + i] = rows_in[2, :, head_columns(first + i)].astype(jnp.float32).T.astype(jnp.bfloat16)
 
         @pl.when(me == 0)
         def _():
-            big_to(k_rot, 0, 0, h, 1).start()
-            big_to(v_turn, 1, 1, h, 1).start()
+            for i in range(GROUP):
+                big_to(k_rot, 0, 0, first + i, 1).start()
+                big_to(v_turn, 1, 1, first + i, 1).start()
 
         @pl.when(me >= 2)
         def _():
-            partial_scores(k_rot[h], q_rot[h], 0, h, True)
-            small_to(0, me - 2, h, 1).start()
+            heads_of = range(GROUP)
+            partial_scores(
+                [k_rot[first + i] for i in heads_of], [q_rot[first + i] for i in heads_of], 0, first, True
+            )
+            for i in heads_of:
+                small_to(0, me - 2, first + i, 1).start()
 
         return carry
 
-    lax.fori_loop(0, count, prepare, 0)
+    lax.fori_loop(0, count // GROUP, prepare, 0)
 
     def lowest(h):
         scores = jnp.where(causal, turned_scores(k_rot[h], q_rot[h]), -1e30)
         _, e, z = exponents(scores)
         finish(mixed(e, 1.0 / z, lam_ref[h], v_turn[h]), h)
 
-    def centre_keys(h):
-        return (
-            jnp.concatenate([big[0, h], k_rot[h]], axis=0),
-            jnp.concatenate([big[1, h], v_turn[h]], axis=1),
-        )
-
-    def served(h, slot, levels, keys, values):
-        top, e, z = exponents(turned_scores(keys, big[slot, h]))
-        level = joined([top + jnp.log2(z)] + levels)
-        big_out[slot - 2, h] = mixed(e, jnp.exp2(top - level), lam_ref[h], values).astype(jnp.bfloat16)
-        put_pair(small_out, slot - 2, h, level)
-
-    def centre_second(h):
-        big_in(0, h)
-        big_in(1, h)
-        big_in(2, h)
-        small_in(0, h)
-        keys, values = centre_keys(h)
-        served(h, 2, [get_pair(small, 0, h)], keys, values)
-        scores = turned_scores(keys, q_rot[h])
-        scores = jnp.concatenate([scores[:tok], jnp.where(causal, scores[tok:], -1e30)], axis=0)
-        _, e, z = exponents(scores)
-        finish(mixed(e, 1.0 / z, lam_ref[h], values), h)
+    def centre(h):
+        for slot in range(4):
+            big_in(slot, h)
+        for slot in range(3):
+            small_in(slot, h)
+        keys = jnp.concatenate([big[0, h], k_rot[h]], axis=0)
+        values = jnp.concatenate([big[1, h], v_turn[h]], axis=1)
+        second, third, third_too = (get_pair(small, slot, h) for slot in range(3))
+        lam = lam_ref[h]
+        pair = 2 * tok
+        scores = turned_scores(keys, q_rot[h], big[2, h], big[3, h])
+        seen = jnp.concatenate([scores[:tok, :pair], jnp.where(causal, scores[tok:, :pair], -1e30)], axis=0)
+        scores = jnp.concatenate([seen, scores[:, pair:]], axis=1)
+        top, e, z = exponents(scores)
+        level = top + jnp.log2(z)
+        level_two = joined([level[:, pair : 2 * pair], second])
+        level_three = joined([level[:, 2 * pair :], third, third_too])
+        put_pair(small_out, 0, h, level_two)
+        put_pair(small_out, 1, h, level_three)
+        scales = [
+            1.0 / z[:, :pair],
+            jnp.exp2(top[:, pair : 2 * pair] - level_two),
+            jnp.exp2(top[:, 2 * pair :] - level_three),
+        ]
+        mixing = [mixing_of(e[:, i * pair : (i + 1) * pair], scale, lam) for i, scale in enumerate(scales)]
+        raw = jnp.dot(values, jnp.concatenate(mixing, axis=1), preferred_element_type=jnp.float32)
+        big_out[1, h] = raw[:, 2 * tok :].astype(jnp.bfloat16)
+        big_out[0, h] = raw[:, tok : 2 * tok].astype(jnp.bfloat16)
+        small_to(1, 1, h, 2).start()
+        last_level(h).start()
+        big_to(big_out.at[1], 1, 0, h, 3).start()
+        small_to(0, 0, h, 2).start()
         big_to(big_out.at[0], 0, 0, h, 2).start()
-        small_to(0, 0, h, 2).start()
-
-    def centre_third(h):
-        big_in(3, h)
-        small_in(1, h)
-        small_in(2, h)
-        keys, values = centre_keys(h)
-        served(h, 3, [get_pair(small, 1, h), get_pair(small, 2, h)], keys, values)
-        small_to(1, 1, h, 2).start()
-        big_to(big_out.at[1], 1, 0, h, 3).start()
-        moved(
+        finish(raw[:, :tok], h)
+
+    def last_level(h):
+        return moved(
             small_out.at[1, h], small.at[1, h], small_send.at[2, h], small_recv.at[1, h], {"sp": 3}
-        ).start()
+        )
 
     def upper_scores(h):
         big_in(3, h)
-        partial_scores(k_rot[h], big[3, h], 1, h, False)
+        partial_scores([k_rot[h]], [big[3, h]], 1, h, False)
         small_to(1, 2, h, 1).start()
+
+        @pl.when(h + AHEAD < count)
+        def _():
+            big_to(q_rot, 0, 2, h + AHEAD, 1).start()
 
     def upper_raw(h, slot, level):
         scale = jnp.exp2(get_pair(kept_top, slot, h) - level)
@@ -670,6 +703,10 @@
 
     group = GROUP
     per_chunk = count // chunks
+
+    def leave(index):
+        span = slice(index * cols, (index + 1) * cols)
+        return pltpu.make_async_copy(out_rows.at[:, span], out_ref.at[0, :, span], out_sem.at[index])
 
     def project(g, first, last):
         step = group * width
@@ -686,12 +723,40 @@
             if not first:
                 term = total[:, span] + term
             if last:
-                out_ref[0, :, span] = term.astype(out_ref.dtype)
+                out_rows[:, span] = term.astype(out_ref.dtype)
+                leave(index).start()
             else:
                 total[:, span] = term
 
     groups = count // group
-    late = 2 * group + 1
+
+    def sent(h):
+        @pl.when(me == 0)
+        def _():
+            big_to(k_rot, 0, 0, h, 1).wait_send()
+            big_to(v_turn, 1, 1, h, 1).wait_send()
+
+        @pl.when(me == 1)
+        def _():
+            big_to(big_out.at[0], 0, 0, h, 2).wait_send()
+            big_to(big_out.at[1], 1, 0, h, 3).wait_send()
+            small_to(0, 0, h, 2).wait_send()
+            small_to(1, 1, h, 2).wait_send()
+            last_level(h).wait_send()
+
+        @pl.when(me == 2)
+        def _():
+            big_to(q_rot, 0, 2, h, 1).wait_send()
+            small_to(0, 0, h, 1).wait_send()
+            small_to(1, 2, h, 1).wait_send()
+
+        @pl.when(me == 3)
+        def _():
+            big_to(q_rot, 1, 3, h, 2).wait_send()
+            big_to(q_rot, 0, 3, h, 1).wait_send()
+            small_to(0, 1, h, 1).wait_send()
+
+    first_y = 2 * per_chunk
 
     def step(it, carry):
         @pl.when((me == 0) & (it < count))
@@ -700,15 +765,21 @@
 
         @pl.when((me == 1) & (it < count))
         def _():
-            centre_second(it)
-
-        @pl.when((me == 1) & (it >= 1) & (it <= count))
-        def _():
-            centre_third(it - 1)
+            centre(it)
 
         @pl.when((me == 2) & (it < count))
         def _():
             upper_scores(it)
+
+        turn = lax.rem(it, per_chunk) == 0
+
+        @pl.when(turn & (it < count))
+        def _():
+            forward_x(it // per_chunk)
+
+        @pl.when(turn & (it >= first_y) & (it < first_y + count))
+        def _():
+            forward_y((it - first_y) // per_chunk)
 
         @pl.when((me == 2) & (it >= LAG))
         def _():
@@ -719,20 +790,12 @@
         def _():
             upper_third(it - LAG)
 
-        turn = lax.rem(it, per_chunk) == 0
-
-        @pl.when(turn & (it >= per_chunk) & (it <= count))
-        def _():
-            forward_x(it // per_chunk - 1)
-
-        first_y = 3 * per_chunk
-
-        @pl.when(turn & (it >= first_y))
-        def _():
-            forward_y((it - first_y) // per_chunk)
+        @pl.when(it >= LAG)
+        def _():
+            sent(it - LAG)
 
         for g in range(groups - 1):
-            @pl.when(it == g * group + late)
+            @pl.when(it == (g + 1) * group - 1 + LAG)
             def _(g=g):
                 if g == 0:
                     own_weight.wait()
@@ -740,40 +803,13 @@
 
         return carry
 
-    steps = count + LAG
-    lax.fori_loop(0, steps, step, 0)
-    for r in range((steps - 1 - 3 * per_chunk) // per_chunk + 1, chunks):
-        forward_y(r)
+    lax.fori_loop(0, count + LAG, step, 0)
     project(groups - 1, False, True)
 
     def drain(h, carry):
-        @pl.when(me == 0)
-        def _():
-            big_to(k_rot, 0, 0, h, 1).wait_send()
-            big_to(v_turn, 1, 1, h, 1).wait_send()
-
-        @pl.when(me == 1)
-        def _():
-            big_to(big_out.at[0], 0, 0, h, 2).wait_send()
-            small_to(0, 0, h, 2).wait_send()
-            small_to(1, 1, h, 2).wait_send()
-            big_to(big_out.at[1], 1, 0, h, 3).wait_send()
-            moved(
-                small_out.at[1, h], small.at[1, h], small_send.at[2, h], small_recv.at[1, h], {"sp": 3}
-            ).wait_send()
-
         @pl.when(me == 2)
         def _():
-            big_to(q_rot, 0, 2, h, 1).wait_send()
-            small_to(0, 0, h, 1).wait_send()
-            small_to(1, 2, h, 1).wait_send()
             big_to(big_out.at[1], 1, 1, h, 3).wait_send()
-
-        @pl.when(me == 3)
-        def _():
-            big_to(q_rot, 1, 3, h, 2).wait_send()
-            big_to(q_rot, 0, 3, h, 1).wait_send()
-            small_to(0, 1, h, 1).wait_send()
 
         return carry
 
@@ -791,6 +827,8 @@
         return carry
 
     lax.fori_loop(0, chunks, drain_weights, 0)
+    for index in range(n_dp):
+        leave(index).wait()
 
 
 def split_local(n, n_dp, n_grp, query_rows, key_rows, value_rows, query_gain, key_gain, lambdas, head_gain, out_weight):
@@ -813,7 +851,7 @@
         out_shape=jax.ShapeDtypeStruct((1, tok, n_dp * cols), jnp.bfloat16),
         in_specs=[anywhere] * 3
         + [vmem, vmem, pl.BlockSpec(memory_space=pltpu.SMEM), vmem, anywhere, anywhere, anywhere],
-        out_specs=vmem,
+        out_specs=anywhere,
         scratch_shapes=[
             pltpu.VMEM((tok, n_dp * cols), jnp.float32),
             pltpu.VMEM((3, tok, count * width), jnp.bfloat16),
@@ -831,7 +869,10 @@
             pltpu.VMEM((n_dp, depth, cols), jnp.bfloat16),
             pltpu.VMEM((tok, width), jnp.float32),
             pltpu.VMEM((tok, width), jnp.float32),
+            pltpu.VMEM((4, tok, width), jnp.float32),
+            pltpu.VMEM((tok, n_dp * cols), jnp.bfloat16),
             dma((6,)),
+            dma((n_dp,)),
             dma((2, count)),
             dma((4, count)),
             dma((3, count)),

time: 68.4 us -> 45.2 us (0.66)
  the two profiles are of different devices: /device:TPU:27 before, /device:TPU:30 now
where the time goes in v2:
time: 45.2 us; the launch traced here: 45 us
  Pallas kernels  43.2 us (96%)
  local copies, waits for them, and re-layouts  1.88 us (4%)
    pallas_call x1, Pallas kernels, split_local(): pl.pallas_call(functools.partial(split_kernel, n, n_dp, n_grp, head_size,...  43.2 us
    unnamed x1, local copies, waits for them, and re-layouts  1.88 us

profile of v2, /device:TPU:30, one launch (start us, length us, event | category | flops | bytes accessed | tf_op | source)
XLA Modules:
  0.0 45.0 jit_solution(3447843359233789496)
XLA Ops:
  0.0 43.2 %shard_map.100 = bf16[1,128,2048]{2,1,0:T(8,128)(2,1)} custom-call(bf16[1,128,2048]{2,1,0:T(8,128)(2,1)} %q_in.1, bf16[1,128,2048]{2,1,0:T(8,128)(2,1)} %k_in.1, bf16[1,128,2048]{2,1,0:T(8,128)(2,1)} %v_in.1, f32[1,64]{1,0:T(1,128)} %bitcast.3, f32[1,64]{1,0:T(1,128)} %bitcast.4, f32[16]{0:T(128)} %lam_ref.1, f32[1,128]{1,0:T(1,128)} %bitcast.5, ...), custom_call_target="tpu_custom_call" | custom-call | tf_op jit(solution)/shard_map/pallas_call | solution.py:849
  43.2 1.9 %copy.12 = bf16[1,128,2048]{2,1,0:T(8,128)(2,1)} copy(bf16[1,128,2048]{2,1,0:T(8,128)(2,1)} %shard_map.100) | data formatting | bytes 1048576

commit v3 on v2

--- a/solution.py
+++ b/solution.py
@@ -17,7 +17,10 @@
 PARTS = 4
 GROUP = 4
 LAG = 5
-AHEAD = 2
+AHEAD = 3
+DEEP = 3
+SPREAD = 3
+TALKS = ((0, 1), (1, 2), (1, 3), (2, 3))
 MESH = pl.DeviceIdType.MESH
 
 
@@ -379,9 +382,8 @@
 
 def split_kernel(
     n, n_dp, n_grp, head_size, chunks, q_in, k_in, v_in, qg_ref, kg_ref, lam_ref, hg_ref, w_ref, cos_in, sin_in,
-    out_ref, total, rows_in, q_rot, k_rot, v_turn, big, small, big_out, small_out, kept, kept_top, gain_turn, heads, wfull,
-    cos_ref, sin_ref, turn_ref, out_rows, load_sem, out_sem, big_send, big_recv, small_send, small_recv,
-    wx_send, wx_recv, wy_send, wy_recv, wc_send, wc_recv,
+    out_ref, total, rows_in, rot, v_turn, big, small, big_out, small_out, kept, kept_top, gain_turn, heads, wfull,
+    cos_ref, sin_ref, turn_ref, load_sem, big_send, small_send, came, wx_send, wx_recv, wy_send, wy_recv, wc_send, wc_recv,
 ):
     me = lax.axis_index("sp")
     dp = lax.axis_index("dp")
@@ -390,17 +392,26 @@
     cores = CORES if n_dp % CORES == 0 else 1
     nx = n_dp // cores
     xi, core = dp // cores, lax.rem(dp, cores)
-    count, tok, width = q_rot.shape
+    count, tok, width = v_turn.shape
+    q_rot, k_rot = rot.at[0], rot.at[1]
     depth, cols = w_ref.shape
     piece = depth // (chunks * ways)
+    per_chunk = count // chunks
     factor = head_size ** (-0.5) * math.log2(math.e)
 
     def dp_index(xo, co):
         return lax.rem(xi + xo, nx) * cores + lax.rem(core + co, cores)
 
+    direct = chunks - 1
+    alone = count - GROUP
+
     barrier = pltpu.get_barrier_semaphore()
-    for off in range(1, n):
-        pl.semaphore_signal(barrier, inc=1, device_id={"sp": lax.rem(me + off, n)}, device_id_type=MESH)
+    for here, there in TALKS:
+        for one, other in ((here, there), (there, here)):
+            @pl.when(me == one)
+            def _(other=other):
+                pl.semaphore_signal(barrier, inc=1, device_id={"sp": other}, device_id_type=MESH)
+    talkers = sum(jnp.where((me == here) | (me == there), 1, 0) for here, there in TALKS)
     for xo in range(1, nx):
         pl.semaphore_signal(barrier, inc=1, device_id={"dp": dp_index(xo, 0)}, device_id_type=MESH)
     for co in range(1, cores):
@@ -410,11 +421,11 @@
 
     own = pl.ds(pl.multiple_of(me * tok, tok), tok)
     loads = [
+        pltpu.make_async_copy(cos_in.at[own, :], cos_ref, load_sem.at[3]),
+        pltpu.make_async_copy(sin_in.at[own, :], sin_ref, load_sem.at[4]),
         pltpu.make_async_copy(q_in.at[0], rows_in.at[0], load_sem.at[0]),
         pltpu.make_async_copy(k_in.at[0], rows_in.at[1], load_sem.at[1]),
         pltpu.make_async_copy(v_in.at[0], rows_in.at[2], load_sem.at[2]),
-        pltpu.make_async_copy(cos_in.at[own, :], cos_ref, load_sem.at[3]),
-        pltpu.make_async_copy(sin_in.at[own, :], sin_ref, load_sem.at[4]),
     ]
     own_weight = pltpu.make_async_copy(w_ref, wfull.at[dp], load_sem.at[5])
     for load in loads:
@@ -431,36 +442,40 @@
         first = (r * ways + lax.rem(grp + way, ways)) * piece
         return pl.ds(pl.multiple_of(first, piece), piece)
 
-    def weight_x(xo, r):
-        rows = piece_rows(r, 0)
+    def weight_x(xo, r, way=0):
+        rows = piece_rows(r, way)
         return moved(
-            w_ref.at[rows, :], wfull.at[dp, rows, :], wx_send.at[xo, r], wx_recv.at[xo, r],
+            w_ref.at[rows, :], wfull.at[dp, rows, :], wx_send.at[xo - 1], wx_recv.at[xo - 1, r + way],
             {"dp": dp_index(xo, 0)},
         )
 
-    def weight_x_in(xo, r):
-        block = wfull.at[dp_index(nx - xo, 0), piece_rows(r, 0), :]
-        return moved(block, block, wx_send.at[xo, r], wx_recv.at[xo, r], {"dp": dp_index(xo, 0)})
+    def weight_x_in(xo, r, way=0):
+        block = wfull.at[dp_index(nx - xo, 0), piece_rows(r, way), :]
+        return moved(block, block, wx_send.at[xo - 1], wx_recv.at[xo - 1, r + way], {"dp": dp_index(xo, 0)})
 
     def weight_y(xo, r):
         block = wfull.at[dp_index(nx - xo, 0), piece_rows(r, 0), :]
-        return moved(block, block, wy_send.at[xo, r], wy_recv.at[xo, r], {"grp": lax.rem(grp + 1, ways)})
+        return moved(
+            block, block, wy_send.at[xo - 1], wy_recv.at[xo - 1, r], {"grp": lax.rem(grp + 1, ways)}
+        )
 
     def weight_y_in(xo, r):
         block = wfull.at[dp_index(nx - xo, 0), piece_rows(r, 1), :]
-        return moved(block, block, wy_send.at[xo, r], wy_recv.at[xo, r], {"grp": lax.rem(grp + 1, ways)})
+        return moved(
+            block, block, wy_send.at[xo - 1], wy_recv.at[xo - 1, r], {"grp": lax.rem(grp + 1, ways)}
+        )
 
     def weight_core(xo, r, way):
         rows = piece_rows(r, way)
         target = wfull.at[dp_index(nx - xo, 0), rows, :]
         return moved(
             w_ref.at[rows, :] if xo == 0 else target, target,
-            wc_send.at[xo, r, way], wc_recv.at[xo, r, way], {"dp": dp_index(0, 1)},
-        )
-
-    def weight_core_in(xo, r, way):
-        block = wfull.at[dp_index(nx - xo, 1), piece_rows(r, way), :]
-        return moved(block, block, wc_send.at[xo, r, way], wc_recv.at[xo, r, way], {"dp": dp_index(0, 1)})
+            wc_send.at[xo], wc_recv.at[xo, r * per_chunk // GROUP], {"dp": dp_index(0, 1)},
+        )
+
+    def weight_core_in(xo, g, rows):
+        block = wfull.at[dp_index(nx - xo, 1), rows, :]
+        return moved(block, block, wc_send.at[xo], wc_recv.at[xo, g], {"dp": dp_index(0, 1)})
 
     def forward_x(r):
         for xo in range(1, nx):
@@ -470,6 +485,15 @@
             if cores > 1:
                 weight_core(xo, r, 0).start()
 
+            @pl.when(r + DEEP < direct)
+            def _(xo=xo):
+                weight_x(xo, r + DEEP).start()
+
+            for way in range(ways):
+                @pl.when(r == max(direct - DEEP, 0) + way)
+                def _(xo=xo, way=way):
+                    weight_x(xo, direct, way).start()
+
     def forward_y(r):
         if ways > 1:
             for xo in range(1, nx):
@@ -477,24 +501,28 @@
                 if cores > 1:
                     weight_core(xo, r, 1).start()
 
-    def big_to(source, lane, slot, h, peer):
-        return moved(source.at[h], big.at[slot, h], big_send.at[lane, h], big_recv.at[slot, h], {"sp": peer})
+    def forward_direct():
+        for way in range(ways):
+            for xo in range(1, nx):
+                weight_x_in(xo, direct, way).wait_recv()
+                if cores > 1:
+                    weight_core(xo, direct, way).start()
+
+    def big_to(source, lane, slot, h, peer, what=0):
+        return moved(source.at[h], big.at[h, slot], big_send.at[lane], came.at[what, h], {"sp": peer})
 
     def small_to(lane, slot, h, peer):
-        return moved(
-            small_out.at[lane, h], small.at[slot, h], small_send.at[lane, h], small_recv.at[slot, h], {"sp": peer}
-        )
-
-    def big_in(slot, h):
-        block = big.at[slot, h]
-        moved(block, block, big_send.at[0, h], big_recv.at[slot, h], {"sp": lax.rem(me + 1, n)}).wait_recv()
-
-    def small_in(slot, h):
-        block = small.at[slot, h]
-        moved(block, block, small_send.at[0, h], small_recv.at[slot, h], {"sp": lax.rem(me + 1, n)}).wait_recv()
-
-    pl.semaphore_wait(barrier, (n - 1) + (nx - 1) + (cores - 1) + (ways - 1))
-    for r in range(chunks):
+        source = small_out.at[h, min(lane, 1)]
+        return moved(source, small.at[h, slot], small_send.at[lane], came.at[1, h], {"sp": peer})
+
+    def came_in(block, what, h):
+        moved(block, block, big_send.at[0], came.at[what, h], {"sp": lax.rem(me + 1, n)}).wait_recv()
+
+    def gone(block, sem):
+        moved(block, block, sem, came.at[0, 0], {"sp": lax.rem(me + 1, n)}).wait_send()
+
+    pl.semaphore_wait(barrier, talkers + (nx - 1) + (cores - 1) + (ways - 1))
+    for r in range(min(DEEP, direct)):
         for xo in range(1, nx):
             weight_x(xo, r).start()
     if cores > 1:
@@ -511,7 +539,7 @@
     same_map = jnp.where((down < head_size) == (across < head_size), 1.0, 0.0).astype(jnp.bfloat16)
     sums = jnp.concatenate([same_map, same_map], axis=0)
 
-    def norm_rotate(which, target, first):
+    def norm_rotate(which, first):
         blocks = [rows_in[which, :, head_columns(first + i)] for i in range(GROUP)]
         stacked = jnp.concatenate(blocks, axis=0)
         x = stacked.astype(jnp.float32)
@@ -525,9 +553,9 @@
             part = slice(i * tok, (i + 1) * tok)
             straight = x[part] * inverse[part] * turn_ref[2 * which]
             turned = other[part] * inverse[part] * turn_ref[2 * which + 1]
-            target[first + i] = (straight + turned).astype(jnp.bfloat16)
-
-    for load in loads:
+            rot[which, first + i] = (straight + turned).astype(jnp.bfloat16)
+
+    for load in loads[:3]:
         load.wait()
     gain_turn[...] = jnp.broadcast_to(hg_ref[...], (tok, width)).T
     for which, gain in enumerate((qg_ref, kg_ref)):
@@ -562,12 +590,12 @@
     def mixed(e, scale, lam, values):
         return jnp.dot(values, mixing_of(e, scale, lam), preferred_element_type=jnp.float32)
 
-    def put_pair(ref, first, h, pair):
-        ref[first, h, 0:1, :] = pair[:, :tok]
-        ref[first, h, 1:2, :] = pair[:, tok:]
-
-    def get_pair(ref, first, h):
-        return jnp.concatenate([ref[first, h, 0:1, :], ref[first, h, 1:2, :]], axis=1)
+    def put_pair(ref, h, slot, pair):
+        ref[h, slot, 0:1, :] = pair[:, :tok]
+        ref[h, slot, 1:2, :] = pair[:, tok:]
+
+    def get_pair(ref, h, slot):
+        return jnp.concatenate([ref[h, slot, 0:1, :], ref[h, slot, 1:2, :]], axis=1)
 
     def joined(levels):
         top = functools.reduce(jnp.maximum, levels)
@@ -584,47 +612,88 @@
             scores = [jnp.where(causal, s, -1e30) for s in scores]
         parts = [exponents(s) for s in scores]
         for i, (top, e, z) in enumerate(parts):
-            kept[slot, first + i] = e
-            put_pair(kept_top, slot, first + i, top)
-            put_pair(small_out, slot, first + i, top + jnp.log2(z))
+            kept[first + i, slot] = e
+            put_pair(kept_top, first + i, slot, top)
+            put_pair(small_out, first + i, slot, top + jnp.log2(z))
+
+    def third_queries(h):
+        big_to(q_rot, 1, 3, h, 2).start()
+        big_to(q_rot, 0, 3, h, 1).start()
 
     def prepare(j, carry):
         first = j * GROUP
-        norm_rotate(0, q_rot, first)
-
-        @pl.when(me == 3)
-        def _():
-            for i in range(GROUP):
-                big_to(q_rot, 1, 3, first + i, 2).start()
-                big_to(q_rot, 0, 3, first + i, 1).start()
+        members = range(GROUP)
+
+        @pl.when((me == 0) & (j == 0))
+        def _():
+            loads[3].wait()
+            loads[4].wait()
+
+        def turn_values():
+            for i in members:
+                v_turn[first + i] = rows_in[2, :, head_columns(first + i)].astype(jnp.float32).T.astype(jnp.bfloat16)
+
+        ahead = jnp.where(me == 0, 1, 0)
+        norm_rotate(ahead, first)
+
+        @pl.when((me == 3) & (j == 0))
+        def _():
+            third_queries(0)
 
         @pl.when((me == 2) & (j == 0))
         def _():
             for i in range(AHEAD):
                 big_to(q_rot, 0, 2, i, 1).start()
 
-        norm_rotate(1, k_rot, first)
-        for i in range(GROUP):
-            v_turn[first + i] = rows_in[2, :, head_columns(first + i)].astype(jnp.float32).T.astype(jnp.bfloat16)
+        @pl.when((me > 0) & (j == 0))
+        def _():
+            loads[3].wait()
+            loads[4].wait()
+
+        turn_values()
 
         @pl.when(me == 0)
         def _():
-            for i in range(GROUP):
+            for i in members:
                 big_to(k_rot, 0, 0, first + i, 1).start()
                 big_to(v_turn, 1, 1, first + i, 1).start()
 
-        @pl.when(me >= 2)
-        def _():
-            heads_of = range(GROUP)
-            partial_scores(
-                [k_rot[first + i] for i in heads_of], [q_rot[first + i] for i in heads_of], 0, first, True
-            )
-            for i in heads_of:
-                small_to(0, me - 2, first + i, 1).start()
+        norm_rotate(1 - ahead, first)
+
+        @pl.when((me == 2) & (first >= alone))
+        def _():
+            for i in members:
+                big_to(k_rot, 2, 2, first + i, 3, 2).start()
+                big_to(v_turn, 2, 3, first + i, 3, 2).start()
+
+        @pl.when((me == 2) | ((me == 3) & (first < alone)))
+        def _():
+            partial_scores([k_rot[first + i] for i in members], [q_rot[first + i] for i in members], 0, first, True)
+
+        @pl.when(me == 2)
+        def _():
+            for i in members:
+                small_to(0, 0, first + i, 1).start()
+
+        @pl.when((me == 3) & (first < alone))
+        def _():
+            for i in members:
+                if i:
+                    third_queries(first + i)
+                else:
+                    @pl.when(j > 0)
+                    def _():
+                        third_queries(first)
+                small_to(0, 1, first + i, 1).start()
 
         return carry
 
     lax.fori_loop(0, count // GROUP, prepare, 0)
+
+    @pl.when(me == 1)
+    def _():
+        for h in range(alone, count):
+            small[h, 2] = jnp.full((2, tok), -1e30, jnp.float32)
 
     def lowest(h):
         scores = jnp.where(causal, turned_scores(k_rot[h], q_rot[h]), -1e30)
@@ -632,24 +701,30 @@
         finish(mixed(e, 1.0 / z, lam_ref[h], v_turn[h]), h)
 
     def centre(h):
-        for slot in range(4):
-            big_in(slot, h)
-        for slot in range(3):
-            small_in(slot, h)
-        keys = jnp.concatenate([big[0, h], k_rot[h]], axis=0)
-        values = jnp.concatenate([big[1, h], v_turn[h]], axis=1)
-        second, third, third_too = (get_pair(small, slot, h) for slot in range(3))
+        came_in(big.at[h], 0, h)
+
+        @pl.when(h < alone)
+        def _():
+            came_in(small.at[h], 1, h)
+
+        @pl.when(h >= alone)
+        def _():
+            came_in(small.at[h, 0:2], 1, h)
+
+        keys = jnp.concatenate([big[h, 0], k_rot[h]], axis=0)
+        values = jnp.concatenate([big[h, 1], v_turn[h]], axis=1)
+        second, third, third_too = (get_pair(small, h, slot) for slot in range(3))
         lam = lam_ref[h]
         pair = 2 * tok
-        scores = turned_scores(keys, q_rot[h], big[2, h], big[3, h])
+        scores = turned_scores(keys, q_rot[h], big[h, 2], big[h, 3])
         seen = jnp.concatenate([scores[:tok, :pair], jnp.where(causal, scores[tok:, :pair], -1e30)], axis=0)
         scores = jnp.concatenate([seen, scores[:, pair:]], axis=1)
         top, e, z = exponents(scores)
         level = top + jnp.log2(z)
         level_two = joined([level[:, pair : 2 * pair], second])
         level_three = joined([level[:, 2 * pair :], third, third_too])
-        put_pair(small_out, 0, h, level_two)
-        put_pair(small_out, 1, h, level_three)
+        put_pair(small_out, h, 0, level_two)
+        put_pair(small_out, h, 1, level_three)
         scales = [
             1.0 / z[:, :pair],
             jnp.exp2(top[:, pair : 2 * pair] - level_two),
@@ -659,63 +734,90 @@
         raw = jnp.dot(values, jnp.concatenate(mixing, axis=1), preferred_element_type=jnp.float32)
         big_out[1, h] = raw[:, 2 * tok :].astype(jnp.bfloat16)
         big_out[0, h] = raw[:, tok : 2 * tok].astype(jnp.bfloat16)
-        small_to(1, 1, h, 2).start()
-        last_level(h).start()
+
+        @pl.when(h < alone)
+        def _():
+            small_to(1, 1, h, 2).start()
+
+        small_to(0, 0, h, 2).start()
+        small_to(2, 1, h, 3).start()
         big_to(big_out.at[1], 1, 0, h, 3).start()
-        small_to(0, 0, h, 2).start()
-        big_to(big_out.at[0], 0, 0, h, 2).start()
+        big_to(big_out.at[0], 0, 0, h, 2, 2).start()
         finish(raw[:, :tok], h)
 
-    def last_level(h):
-        return moved(
-            small_out.at[1, h], small.at[1, h], small_send.at[2, h], small_recv.at[1, h], {"sp": 3}
-        )
-
     def upper_scores(h):
-        big_in(3, h)
-        partial_scores([k_rot[h]], [big[3, h]], 1, h, False)
-        small_to(1, 2, h, 1).start()
-
-        @pl.when(h + AHEAD < count)
+        @pl.when(h < alone)
+        def _():
+            came_in(big.at[h, 3], 0, h)
+            partial_scores([k_rot[h]], [big[h, 3]], 1, h, False)
+            small_to(1, 2, h, 1).start()
+
+        @pl.when(h + AHEAD < alone)
         def _():
             big_to(q_rot, 0, 2, h + AHEAD, 1).start()
 
+        @pl.when(h == alone - 2)
+        def _():
+            big_to(q_rot, 0, 2, alone, 1).start()
+
+        @pl.when(h == alone - 1)
+        def _():
+            for i in range(1, GROUP):
+                big_to(q_rot, 0, 2, alone + i, 1).start()
+
     def upper_raw(h, slot, level):
-        scale = jnp.exp2(get_pair(kept_top, slot, h) - level)
-        return mixed(kept[slot, h], scale, lam_ref[h], v_turn[h])
-
-    def upper_help(h):
-        small_in(1, h)
-        big_out[1, h] = upper_raw(h, 1, get_pair(small, 1, h)).astype(jnp.bfloat16)
-        big_to(big_out.at[1], 1, 1, h, 3).start()
+        scale = jnp.exp2(get_pair(kept_top, h, slot) - level)
+        return mixed(kept[h, slot], scale, lam_ref[h], v_turn[h])
 
     def upper_second(h):
-        big_in(0, h)
-        small_in(0, h)
-        finish(upper_raw(h, 0, get_pair(small, 0, h)) + big[0, h].astype(jnp.float32), h)
+        @pl.when(h < alone)
+        def _():
+            came_in(small.at[h, 0:2], 1, h)
+            big_out[1, h] = upper_raw(h, 1, get_pair(small, h, 1)).astype(jnp.bfloat16)
+            big_to(big_out.at[1], 1, 1, h, 3).start()
+
+        @pl.when(h >= alone)
+        def _():
+            came_in(small.at[h, 0:1], 1, h)
+
+        came_in(big.at[h, 0], 2, h)
+        finish(upper_raw(h, 0, get_pair(small, h, 0)) + big[h, 0].astype(jnp.float32), h)
+
+    def joint_scores(h):
+        came_in(big.at[h, 2:4], 2, h)
+        scores = turned_scores(jnp.concatenate([big[h, 2], k_rot[h]], axis=0), q_rot[h])
+        scores = jnp.concatenate([scores[:tok], jnp.where(causal, scores[tok:], -1e30)], axis=0)
+        top, e, z = exponents(scores)
+        kept[h, 0] = e[:tok]
+        kept[h, 1] = e[tok:]
+        put_pair(kept_top, h, 0, top)
+        put_pair(small_out, h, 0, top + jnp.log2(z))
 
     def upper_third(h):
-        big_in(0, h)
-        small_in(1, h)
-        big_in(1, h)
-        raw = upper_raw(h, 0, get_pair(small, 1, h)) + big[0, h].astype(jnp.float32)
-        finish(raw + big[1, h].astype(jnp.float32), h)
+        came_in(small.at[h, 1], 1, h)
+
+        @pl.when(h < alone)
+        def _():
+            came_in(big.at[h, 0:2], 0, h)
+            raw = upper_raw(h, 0, get_pair(small, h, 1)) + big[h, 0].astype(jnp.float32)
+            finish(raw + big[h, 1].astype(jnp.float32), h)
+
+        @pl.when(h >= alone)
+        def _():
+            came_in(big.at[h, 0], 0, h)
+            scale = jnp.exp2(get_pair(kept_top, h, 0) - get_pair(small, h, 1))
+            e = jnp.concatenate([kept[h, 0], kept[h, 1]], axis=0)
+            values = jnp.concatenate([big[h, 3], v_turn[h]], axis=1)
+            finish(mixed(e, scale, lam_ref[h], values) + big[h, 0].astype(jnp.float32), h)
 
     group = GROUP
-    per_chunk = count // chunks
-
-    def leave(index):
-        span = slice(index * cols, (index + 1) * cols)
-        return pltpu.make_async_copy(out_rows.at[:, span], out_ref.at[0, :, span], out_sem.at[index])
 
     def project(g, first, last):
         step = group * width
         rows = pl.ds(g * step, step) if isinstance(g, int) else pl.ds(pl.multiple_of(g * step, step), step)
         if cores > 1:
             for xo in range(nx):
-                for r in range(group // per_chunk):
-                    for way in range(ways):
-                        weight_core_in(xo, g * (group // per_chunk) + r, way).wait_recv()
+                weight_core_in(xo, g, rows).wait_recv()
         block = heads[:, rows]
         for index in range(n_dp):
             term = jnp.dot(block, wfull[index, rows, :], preferred_element_type=jnp.float32)
@@ -723,42 +825,35 @@
             if not first:
                 term = total[:, span] + term
             if last:
-                out_rows[:, span] = term.astype(out_ref.dtype)
-                leave(index).start()
+                out_ref[0, :, span] = term.astype(out_ref.dtype)
             else:
                 total[:, span] = term
 
     groups = count // group
 
-    def sent(h):
-        @pl.when(me == 0)
-        def _():
-            big_to(k_rot, 0, 0, h, 1).wait_send()
-            big_to(v_turn, 1, 1, h, 1).wait_send()
-
-        @pl.when(me == 1)
-        def _():
-            big_to(big_out.at[0], 0, 0, h, 2).wait_send()
-            big_to(big_out.at[1], 1, 0, h, 3).wait_send()
-            small_to(0, 0, h, 2).wait_send()
-            small_to(1, 1, h, 2).wait_send()
-            last_level(h).wait_send()
-
-        @pl.when(me == 2)
-        def _():
-            big_to(q_rot, 0, 2, h, 1).wait_send()
-            small_to(0, 0, h, 1).wait_send()
-            small_to(1, 2, h, 1).wait_send()
-
-        @pl.when(me == 3)
-        def _():
-            big_to(q_rot, 1, 3, h, 2).wait_send()
-            big_to(q_rot, 0, 3, h, 1).wait_send()
-            small_to(0, 1, h, 1).wait_send()
-
-    first_y = 2 * per_chunk
+    first_x = jnp.where(me == 1, 0, 1)
+    first_y = first_x + 2 * per_chunk
+    last_x = first_x + direct * per_chunk
 
     def step(it, carry):
+        @pl.when((me == 2) & (it < count))
+        def _():
+            upper_scores(it)
+
+        turn = lax.rem(it - first_x + per_chunk, per_chunk) == 0
+
+        @pl.when(turn & (it >= first_x) & (it < last_x))
+        def _():
+            forward_x((it - first_x) // per_chunk)
+
+        @pl.when(turn & (it >= first_y) & (it < first_y + direct * per_chunk))
+        def _():
+            forward_y((it - first_y) // per_chunk)
+
+        @pl.when(it == jnp.where(me == 1, count, last_x))
+        def _():
+            forward_direct()
+
         @pl.when((me == 0) & (it < count))
         def _():
             lowest(it)
@@ -767,35 +862,26 @@
         def _():
             centre(it)
 
-        @pl.when((me == 2) & (it < count))
-        def _():
-            upper_scores(it)
-
-        turn = lax.rem(it, per_chunk) == 0
-
-        @pl.when(turn & (it < count))
-        def _():
-            forward_x(it // per_chunk)
-
-        @pl.when(turn & (it >= first_y) & (it < first_y + count))
-        def _():
-            forward_y((it - first_y) // per_chunk)
+        @pl.when((me == 3) & (it < GROUP))
+        def _():
+            joint_scores(alone + it)
 
         @pl.when((me == 2) & (it >= LAG))
         def _():
-            upper_help(it - LAG)
             upper_second(it - LAG)
 
+        @pl.when((me == 3) & (it >= LAG + SPREAD) & (it < LAG + SPREAD + GROUP))
+        def _():
+            h = alone + it - (LAG + SPREAD)
+            big_to(q_rot, 0, 3, h, 1).start()
+            small_to(0, 1, h, 1).start()
+
         @pl.when((me == 3) & (it >= LAG))
         def _():
             upper_third(it - LAG)
 
-        @pl.when(it >= LAG)
-        def _():
-            sent(it - LAG)
-
         for g in range(groups - 1):
-            @pl.when(it == (g + 1) * group - 1 + LAG)
+            @pl.when(it == (g + 1) * group + 1 + jnp.where(me == 1, LAG - 2, LAG))
             def _(g=g):
                 if g == 0:
                     own_weight.wait()
@@ -806,29 +892,47 @@
     lax.fori_loop(0, count + LAG, step, 0)
     project(groups - 1, False, True)
 
-    def drain(h, carry):
-        @pl.when(me == 2)
-        def _():
-            big_to(big_out.at[1], 1, 1, h, 3).wait_send()
-
-        return carry
-
-    lax.fori_loop(0, count, drain, 0)
-
-    def drain_weights(r, carry):
-        for xo in range(nx):
-            if xo:
-                weight_x(xo, r).wait_send()
-                if ways > 1:
-                    weight_y(xo, r).wait_send()
-            if cores > 1:
-                for way in range(ways):
-                    weight_core(xo, r, way).wait_send()
-        return carry
-
-    lax.fori_loop(0, chunks, drain_weights, 0)
-    for index in range(n_dp):
-        leave(index).wait()
+    whole, most = q_rot.at[:], q_rot.at[0:alone]
+    rows = small_out.at[:, 0]
+    most_rows = small_out.at[0:alone, 0]
+
+    @pl.when(me == 0)
+    def _():
+        gone(whole, big_send.at[0])
+        gone(whole, big_send.at[1])
+
+    @pl.when(me == 1)
+    def _():
+        gone(whole, big_send.at[0])
+        gone(whole, big_send.at[1])
+        gone(rows, small_send.at[0])
+        gone(most_rows, small_send.at[1])
+        gone(rows, small_send.at[2])
+
+    @pl.when(me == 2)
+    def _():
+        gone(whole, big_send.at[0])
+        gone(most, big_send.at[1])
+        gone(q_rot.at[0 : 2 * GROUP], big_send.at[2])
+        gone(rows, small_send.at[0])
+        gone(most_rows, small_send.at[1])
+
+    @pl.when(me == 3)
+    def _():
+        gone(whole, big_send.at[0])
+        gone(most, big_send.at[1])
+        gone(rows, small_send.at[0])
+
+    for xo in range(nx):
+        if xo:
+            sent_x = wfull.at[0, 0 : (direct + ways) * piece, :]
+            moved(sent_x, sent_x, wx_send.at[xo - 1], wx_recv.at[0, 0], {"dp": dp_index(xo, 0)}).wait_send()
+            if ways > 1:
+                sent_y = wfull.at[0, 0 : direct * piece, :]
+                moved(sent_y, sent_y, wy_send.at[xo - 1], wy_recv.at[0, 0], {"dp": dp_index(xo, 0)}).wait_send()
+        if cores > 1:
+            sent_core = wfull.at[0]
+            moved(sent_core, sent_core, wc_send.at[xo], wc_recv.at[0, 0], {"dp": dp_index(0, 1)}).wait_send()
 
 
 def split_local(n, n_dp, n_grp, query_rows, key_rows, value_rows, query_gain, key_gain, lambdas, head_gain, out_weight):
@@ -845,44 +949,40 @@
     anywhere = pl.BlockSpec(memory_space=pl.ANY)
     vmem = pl.BlockSpec(memory_space=pltpu.VMEM)
     dma = pltpu.SemaphoreType.DMA
-    block = (count, tok, width)
+    across = max(nx - 1, 1)
     return pl.pallas_call(
         functools.partial(split_kernel, n, n_dp, n_grp, head_size, chunks),
-        out_shape=jax.ShapeDtypeStruct((1, tok, n_dp * cols), jnp.bfloat16),
+        out_shape=pltpu.VMEM((1, tok, n_dp * cols), jnp.bfloat16),
         in_specs=[anywhere] * 3
         + [vmem, vmem, pl.BlockSpec(memory_space=pltpu.SMEM), vmem, anywhere, anywhere, anywhere],
-        out_specs=anywhere,
+        out_specs=vmem,
         scratch_shapes=[
             pltpu.VMEM((tok, n_dp * cols), jnp.float32),
             pltpu.VMEM((3, tok, count * width), jnp.bfloat16),
-            pltpu.VMEM(block, jnp.bfloat16),
-            pltpu.VMEM(block, jnp.bfloat16),
-            pltpu.VMEM(block, jnp.bfloat16),
-            pltpu.VMEM((4,) + block, jnp.bfloat16),
-            pltpu.VMEM((3, count, 2, tok), jnp.float32),
-            pltpu.VMEM((2,) + block, jnp.bfloat16),
-            pltpu.VMEM((2, count, 2, tok), jnp.float32),
-            pltpu.VMEM((2, count, tok, 2 * tok), jnp.float32),
-            pltpu.VMEM((2, count, 2, tok), jnp.float32),
+            pltpu.VMEM((2, count, tok, width), jnp.bfloat16),
+            pltpu.VMEM((count, tok, width), jnp.bfloat16),
+            pltpu.VMEM((count, 4, tok, width), jnp.bfloat16),
+            pltpu.VMEM((count, 3, 2, tok), jnp.float32),
+            pltpu.VMEM((2, count, tok, width), jnp.bfloat16),
+            pltpu.VMEM((count, 2, 2, tok), jnp.float32),
+            pltpu.VMEM((count, 2, tok, 2 * tok), jnp.float32),
+            pltpu.VMEM((count, 2, 2, tok), jnp.float32),
             pltpu.VMEM((width, tok), jnp.float32),
             pltpu.VMEM((tok, count * width), jnp.bfloat16),
             pltpu.VMEM((n_dp, depth, cols), jnp.bfloat16),
             pltpu.VMEM((tok, width), jnp.float32),
             pltpu.VMEM((tok, width), jnp.float32),
             pltpu.VMEM((4, tok, width), jnp.float32),
-            pltpu.VMEM((tok, n_dp * cols), jnp.bfloat16),
             dma((6,)),
-            dma((n_dp,)),
-            dma((2, count)),
-            dma((4, count)),
+            dma((3,)),
+            dma((3,)),
             dma((3, count)),
-            dma((3, count)),
-            dma((nx, chunks)),
-            dma((nx, chunks)),
-            dma((nx, chunks)),
-            dma((nx, chunks)),
-            dma((nx, chunks, ways)),
-            dma((nx, chunks, ways)),
+            dma((across,)),
+            dma((across, chunks - 1 + ways)),
+            dma((across,)),
+            dma((across, chunks)),
+            dma((nx,)),
+            dma((nx, count // GROUP)),
         ],
         compiler_params=pltpu.CompilerParams(
             collective_id=0, has_side_effects=True, vmem_limit_bytes=56 * 1024 * 1024

time: 45.2 us -> 38.1 us (0.84)
  Pallas kernels: 43.2 us -> 36.8 us
  local copies, waits for them, and re-layouts: 1.88 us -> 0.8 us
    pallas_call x1, Pallas kernels: 43.2 us -> 36.8 us  [split_local(): pl.pallas_call(functools.partial(split_kernel, n, n_dp, n_grp, head_size,...]
    unnamed x1, local copies, waits for them, and re-layouts: 1.88 us -> 0.8 us
where the time goes in v3:
time: 38.1 us; the launch traced here: 37.6 us
  Pallas kernels  36.8 us (97%)
  local copies, waits for them, and re-layouts  0.8 us (2%)
    pallas_call x1, Pallas kernels, split_local(): pl.pallas_call(functools.partial(split_kernel, n, n_dp, n_grp, head_size,...  36.8 us
    unnamed x1, local copies, waits for them, and re-layouts  0.8 us

profile of v3, /device:TPU:30, one launch (start us, length us, event | category | flops | bytes accessed | tf_op | source)
XLA Modules:
  0.0 37.6 jit_solution(15392895858892606055)
XLA Ops:
  0.0 36.8 %shard_map.100 = bf16[1,128,2048]{2,1,0:T(8,128)(2,1)S(1)} custom-call(bf16[1,128,2048]{2,1,0:T(8,128)(2,1)} %q_in.1, bf16[1,128,2048]{2,1,0:T(8,128)(2,1)} %k_in.1, bf16[1,128,2048]{2,1,0:T(8,128)(2,1)} %v_in.1, f32[1,64]{1,0:T(1,128)} %bitcast.3, f32[1,64]{1,0:T(1,128)} %bitcast.4, f32[16]{0:T(128)} %lam_ref.1, f32[1,128]{1,0:T(1,128)} %bitcast.5, ...), custom_call_target="tpu_custom_call" | custom-call | tf_op jit(solution)/shard_map/pallas_call | solution.py:953
  36.8 0.8 %copy.12 = bf16[1,128,2048]{2,1,0:T(8,128)(2,1)} copy(bf16[1,128,2048]{2,1,0:T(8,128)(2,1)S(1)} %shard_map.100) | data formatting | bytes 1048576

commit v4 on v3

--- a/solution.py
+++ b/solution.py
@@ -16,10 +16,16 @@
 WAYS = 2
 PARTS = 4
 GROUP = 4
-LAG = 5
+LAG = 7
 AHEAD = 3
 DEEP = 3
-SPREAD = 3
+SPREAD = 4
+BEHIND = 2
+NEAR = 4
+HELP = 5
+PROJECT = 10
+SWAP = 2
+PACED = 2
 TALKS = ((0, 1), (1, 2), (1, 3), (2, 3))
 MESH = pl.DeviceIdType.MESH
 
@@ -381,9 +387,9 @@
 
 
 def split_kernel(
-    n, n_dp, n_grp, head_size, chunks, q_in, k_in, v_in, qg_ref, kg_ref, lam_ref, hg_ref, w_ref, cos_in, sin_in,
+    n, n_dp, n_grp, head_size, chunks, q_in, k_in, v_in, qg_in, kg_in, lam_in, hg_in, w_ref, cos_in, sin_in,
     out_ref, total, rows_in, rot, v_turn, big, small, big_out, small_out, kept, kept_top, gain_turn, heads, wfull,
-    cos_ref, sin_ref, turn_ref, load_sem, big_send, small_send, came, wx_send, wx_recv, wy_send, wy_recv, wc_send, wc_recv,
+    cos_ref, sin_ref, turn_ref, qg_ref, kg_ref, lam_ref, hg_ref, load_sem, big_send, small_send, came, wx_send, wx_recv, wy_send, wy_recv, wc_send, wc_recv,
 ):
     me = lax.axis_index("sp")
     dp = lax.axis_index("dp")
@@ -421,6 +427,10 @@
 
     own = pl.ds(pl.multiple_of(me * tok, tok), tok)
     loads = [
+        pltpu.make_async_copy(qg_in, qg_ref, load_sem.at[6]),
+        pltpu.make_async_copy(kg_in, kg_ref, load_sem.at[7]),
+        pltpu.make_async_copy(hg_in, hg_ref, load_sem.at[8]),
+        pltpu.make_async_copy(lam_in, lam_ref, load_sem.at[9]),
         pltpu.make_async_copy(cos_in.at[own, :], cos_ref, load_sem.at[3]),
         pltpu.make_async_copy(sin_in.at[own, :], sin_ref, load_sem.at[4]),
         pltpu.make_async_copy(q_in.at[0], rows_in.at[0], load_sem.at[0]),
@@ -511,24 +521,15 @@
     def big_to(source, lane, slot, h, peer, what=0):
         return moved(source.at[h], big.at[h, slot], big_send.at[lane], came.at[what, h], {"sp": peer})
 
-    def small_to(lane, slot, h, peer):
+    def small_to(lane, slot, h, peer, what):
         source = small_out.at[h, min(lane, 1)]
-        return moved(source, small.at[h, slot], small_send.at[lane], came.at[1, h], {"sp": peer})
+        return moved(source, small.at[h, slot], small_send.at[lane], came.at[what, h], {"sp": peer})
 
     def came_in(block, what, h):
         moved(block, block, big_send.at[0], came.at[what, h], {"sp": lax.rem(me + 1, n)}).wait_recv()
 
     def gone(block, sem):
         moved(block, block, sem, came.at[0, 0], {"sp": lax.rem(me + 1, n)}).wait_send()
-
-    pl.semaphore_wait(barrier, talkers + (nx - 1) + (cores - 1) + (ways - 1))
-    for r in range(min(DEEP, direct)):
-        for xo in range(1, nx):
-            weight_x(xo, r).start()
-    if cores > 1:
-        for r in range(chunks):
-            for way in range(ways):
-                weight_core(0, r, way).start()
 
     lane = lax.broadcasted_iota(jnp.int32, (1, width), 1)
     low_map = lane < head_size
@@ -555,7 +556,7 @@
             turned = other[part] * inverse[part] * turn_ref[2 * which + 1]
             rot[which, first + i] = (straight + turned).astype(jnp.bfloat16)
 
-    for load in loads[:3]:
+    for load in loads[:7]:
         load.wait()
     gain_turn[...] = jnp.broadcast_to(hg_ref[...], (tok, width)).T
     for which, gain in enumerate((qg_ref, kg_ref)):
@@ -618,23 +619,26 @@
 
     def third_queries(h):
         big_to(q_rot, 1, 3, h, 2).start()
-        big_to(q_rot, 0, 3, h, 1).start()
-
-    def prepare(j, carry):
+        big_to(q_rot, 0, 3, h, 1, 2).start()
+
+    members = range(GROUP)
+    ahead = jnp.where(me == 0, 1, 0)
+
+    def begin(j, carry):
         first = j * GROUP
-        members = range(GROUP)
-
-        @pl.when((me == 0) & (j == 0))
-        def _():
-            loads[3].wait()
-            loads[4].wait()
-
-        def turn_values():
-            for i in members:
-                v_turn[first + i] = rows_in[2, :, head_columns(first + i)].astype(jnp.float32).T.astype(jnp.bfloat16)
-
-        ahead = jnp.where(me == 0, 1, 0)
+
+        @pl.when(j == 0)
+        def _():
+            loads[7].wait()
+            loads[8].wait()
+
         norm_rotate(ahead, first)
+        for i in members:
+            v_turn[first + i] = rows_in[2, :, head_columns(first + i)].astype(jnp.float32).T.astype(jnp.bfloat16)
+        return carry
+
+    def spread(j, carry):
+        first = j * GROUP
 
         @pl.when((me == 3) & (j == 0))
         def _():
@@ -642,15 +646,7 @@
 
         @pl.when((me == 2) & (j == 0))
         def _():
-            for i in range(AHEAD):
-                big_to(q_rot, 0, 2, i, 1).start()
-
-        @pl.when((me > 0) & (j == 0))
-        def _():
-            loads[3].wait()
-            loads[4].wait()
-
-        turn_values()
+            big_to(q_rot, 0, 2, 0, 1).start()
 
         @pl.when(me == 0)
         def _():
@@ -673,7 +669,12 @@
         @pl.when(me == 2)
         def _():
             for i in members:
-                small_to(0, 0, first + i, 1).start()
+                small_to(0, 0, first + i, 1, 1).start()
+
+        @pl.when((me == 2) & (j == 0))
+        def _():
+            for i in range(1, AHEAD):
+                big_to(q_rot, 0, 2, i, 1).start()
 
         @pl.when((me == 3) & (first < alone))
         def _():
@@ -684,11 +685,22 @@
                     @pl.when(j > 0)
                     def _():
                         third_queries(first)
-                small_to(0, 1, first + i, 1).start()
+                small_to(0, 1, first + i, 1, 3).start()
 
         return carry
 
-    lax.fori_loop(0, count // GROUP, prepare, 0)
+    lax.fori_loop(0, 1, begin, 0)
+    pl.semaphore_wait(barrier, talkers + (nx - 1) + (cores - 1) + (ways - 1))
+    for r in range(min(DEEP, direct)):
+        for xo in range(1, nx):
+            weight_x(xo, r).start()
+    if cores > 1:
+        for r in range(chunks):
+            for way in range(ways):
+                weight_core(0, r, way).start()
+
+    lax.fori_loop(0, 1, spread, 0)
+    lax.fori_loop(1, count // GROUP, lambda j, carry: spread(j, begin(j, carry)), 0)
 
     @pl.when(me == 1)
     def _():
@@ -700,86 +712,84 @@
         _, e, z = exponents(scores)
         finish(mixed(e, 1.0 / z, lam_ref[h], v_turn[h]), h)
 
-    def centre(h):
-        came_in(big.at[h], 0, h)
-
-        @pl.when(h < alone)
-        def _():
-            came_in(small.at[h], 1, h)
-
-        @pl.when(h >= alone)
-        def _():
-            came_in(small.at[h, 0:2], 1, h)
-
-        keys = jnp.concatenate([big[h, 0], k_rot[h]], axis=0)
-        values = jnp.concatenate([big[h, 1], v_turn[h]], axis=1)
-        second, third, third_too = (get_pair(small, h, slot) for slot in range(3))
-        lam = lam_ref[h]
+    def centre(h, third):
+        if h is not None:
+            came_in(big.at[h, 0:3], 0, h)
+            came_in(small.at[h, 0], 1, h)
+        if third is not None:
+            came_in(big.at[third, 3], 2, third)
+
+            @pl.when(third < alone)
+            def _():
+                came_in(small.at[third, 1:3], 3, third)
+
+            @pl.when(third >= alone)
+            def _():
+                came_in(small.at[third, 1], 3, third)
+
         pair = 2 * tok
-        scores = turned_scores(keys, q_rot[h], big[h, 2], big[h, 3])
-        seen = jnp.concatenate([scores[:tok, :pair], jnp.where(causal, scores[tok:, :pair], -1e30)], axis=0)
-        scores = jnp.concatenate([seen, scores[:, pair:]], axis=1)
-        top, e, z = exponents(scores)
-        level = top + jnp.log2(z)
-        level_two = joined([level[:, pair : 2 * pair], second])
-        level_three = joined([level[:, 2 * pair :], third, third_too])
-        put_pair(small_out, h, 0, level_two)
-        put_pair(small_out, h, 1, level_three)
-        scales = [
-            1.0 / z[:, :pair],
-            jnp.exp2(top[:, pair : 2 * pair] - level_two),
-            jnp.exp2(top[:, 2 * pair :] - level_three),
-        ]
-        mixing = [mixing_of(e[:, i * pair : (i + 1) * pair], scale, lam) for i, scale in enumerate(scales)]
-        raw = jnp.dot(values, jnp.concatenate(mixing, axis=1), preferred_element_type=jnp.float32)
-        big_out[1, h] = raw[:, 2 * tok :].astype(jnp.bfloat16)
-        big_out[0, h] = raw[:, tok : 2 * tok].astype(jnp.bfloat16)
-
-        @pl.when(h < alone)
-        def _():
-            small_to(1, 1, h, 2).start()
-
-        small_to(0, 0, h, 2).start()
-        small_to(2, 1, h, 3).start()
-        big_to(big_out.at[1], 1, 0, h, 3).start()
-        big_to(big_out.at[0], 0, 0, h, 2, 2).start()
-        finish(raw[:, :tok], h)
+        scores, levels, places, values = [], [], [], []
+        for place, x in ((1, h), (2, h), (3, third)):
+            if x is None:
+                continue
+            keys = jnp.concatenate([big[x, 0], k_rot[x]], axis=0)
+            values.append(jnp.concatenate([big[x, 1], v_turn[x]], axis=1))
+            part = turned_scores(keys, q_rot[x] if place == 1 else big[x, place])
+            if place == 1:
+                part = jnp.concatenate([part[:tok], jnp.where(causal, part[tok:], -1e30)], axis=0)
+            scores.append(part)
+            levels.append([get_pair(small, x, slot) for slot in ((), (0,), (1, 2))[place - 1]])
+            places.append((place, x))
+        parts = [exponents(part) for part in scores]
+        scales = []
+        for (place, x), (top, e, z), others in zip(places, parts, levels):
+            if place == 1:
+                scales.append(1.0 / z)
+            else:
+                level = joined([top + jnp.log2(z)] + others)
+                put_pair(small_out, x, place - 2, level)
+                scales.append(jnp.exp2(top - level))
+        mixing = [mixing_of(e, scale, lam_ref[x]) for (_, x), (_, e, _), scale in zip(places, parts, scales)]
+        raws = [jnp.dot(v, m, preferred_element_type=jnp.float32) for v, m in zip(values, mixing)]
+        for (place, x), raw in zip(places, raws):
+            if place > 1:
+                big_out[place - 2, x] = raw.astype(jnp.bfloat16)
+        if third is not None:
+            @pl.when(third < alone)
+            def _():
+                small_to(1, 1, third, 2, 3).start()
+
+            small_to(2, 1, third, 3, 1).start()
+        if h is not None:
+            small_to(0, 0, h, 2, 1).start()
+        if third is not None:
+            big_to(big_out.at[1], 1, 0, third, 3).start()
+        if h is not None:
+            big_to(big_out.at[0], 0, 0, h, 2, 2).start()
+            finish(raws[0], h)
 
     def upper_scores(h):
         @pl.when(h < alone)
         def _():
             came_in(big.at[h, 3], 0, h)
             partial_scores([k_rot[h]], [big[h, 3]], 1, h, False)
-            small_to(1, 2, h, 1).start()
-
-        @pl.when(h + AHEAD < alone)
+            small_to(1, 2, h, 1, 3).start()
+
+        @pl.when(h + AHEAD < count)
         def _():
             big_to(q_rot, 0, 2, h + AHEAD, 1).start()
-
-        @pl.when(h == alone - 2)
-        def _():
-            big_to(q_rot, 0, 2, alone, 1).start()
-
-        @pl.when(h == alone - 1)
-        def _():
-            for i in range(1, GROUP):
-                big_to(q_rot, 0, 2, alone + i, 1).start()
 
     def upper_raw(h, slot, level):
         scale = jnp.exp2(get_pair(kept_top, h, slot) - level)
         return mixed(kept[h, slot], scale, lam_ref[h], v_turn[h])
 
+    def upper_help(h):
+        came_in(small.at[h, 1], 3, h)
+        big_out[1, h] = upper_raw(h, 1, get_pair(small, h, 1)).astype(jnp.bfloat16)
+        big_to(big_out.at[1], 1, 1, h, 3).start()
+
     def upper_second(h):
-        @pl.when(h < alone)
-        def _():
-            came_in(small.at[h, 0:2], 1, h)
-            big_out[1, h] = upper_raw(h, 1, get_pair(small, h, 1)).astype(jnp.bfloat16)
-            big_to(big_out.at[1], 1, 1, h, 3).start()
-
-        @pl.when(h >= alone)
-        def _():
-            came_in(small.at[h, 0:1], 1, h)
-
+        came_in(small.at[h, 0], 1, h)
         came_in(big.at[h, 0], 2, h)
         finish(upper_raw(h, 0, get_pair(small, h, 0)) + big[h, 0].astype(jnp.float32), h)
 
@@ -831,7 +841,13 @@
 
     groups = count // group
 
-    first_x = jnp.where(me == 1, 0, 1)
+    def turned_order(at):
+        early = (at >= alone - SWAP) & (at < alone)
+        late = (at >= alone) & (at < alone + SWAP)
+        return at + jnp.where(early, SWAP, jnp.where(late, -SWAP, 0))
+
+
+    first_x = jnp.where(me == 1, 2, 1)
     first_y = first_x + 2 * per_chunk
     last_x = first_x + direct * per_chunk
 
@@ -850,7 +866,7 @@
         def _():
             forward_y((it - first_y) // per_chunk)
 
-        @pl.when(it == jnp.where(me == 1, count, last_x))
+        @pl.when(it == jnp.where(me < 2, last_x, HELP + alone + 1))
         def _():
             forward_direct()
 
@@ -858,30 +874,42 @@
         def _():
             lowest(it)
 
-        @pl.when((me == 1) & (it < count))
-        def _():
-            centre(it)
-
-        @pl.when((me == 3) & (it < GROUP))
-        def _():
-            joint_scores(alone + it)
-
-        @pl.when((me == 2) & (it >= LAG))
-        def _():
-            upper_second(it - LAG)
-
-        @pl.when((me == 3) & (it >= LAG + SPREAD) & (it < LAG + SPREAD + GROUP))
-        def _():
-            h = alone + it - (LAG + SPREAD)
-            big_to(q_rot, 0, 3, h, 1).start()
-            small_to(0, 1, h, 1).start()
+        @pl.when((me == 1) & (it < BEHIND))
+        def _():
+            centre(it, None)
+
+        @pl.when((me == 1) & (it >= BEHIND) & (it < count))
+        def _():
+            centre(it, jnp.where(it == count - 1, it - 1, it - BEHIND))
+
+        @pl.when((me == 1) & (it >= count - BEHIND) & (it < count))
+        def _():
+            centre(None, jnp.where(it == count - 1, it, it - 1))
+
+        @pl.when((me == 2) & (it >= HELP) & (it < HELP + alone))
+        def _():
+            upper_help(it - HELP)
+
+        @pl.when((me == 2) & (it >= NEAR) & (it < NEAR + count))
+        def _():
+            upper_second(it - NEAR)
+
+        @pl.when((me == 3) & (it >= GROUP) & (it < 2 * GROUP))
+        def _():
+            joint_scores(alone + it - GROUP)
+
+        for i in range(GROUP):
+            @pl.when((me == 3) & (it == LAG + SPREAD + min(i, PACED)))
+            def _(i=i):
+                big_to(q_rot, 0, 3, alone + i, 1, 2).start()
+                small_to(0, 1, alone + i, 1, 3).start()
 
         @pl.when((me == 3) & (it >= LAG))
         def _():
-            upper_third(it - LAG)
+            upper_third(turned_order(it - LAG))
 
         for g in range(groups - 1):
-            @pl.when(it == (g + 1) * group + 1 + jnp.where(me == 1, LAG - 2, LAG))
+            @pl.when(it == g * group + PROJECT + jnp.where(me == 3, 3, jnp.where((me == 1) & (g == 1), 2, 0)))
             def _(g=g):
                 if g == 0:
                     own_weight.wait()
@@ -954,7 +982,7 @@
         functools.partial(split_kernel, n, n_dp, n_grp, head_size, chunks),
         out_shape=pltpu.VMEM((1, tok, n_dp * cols), jnp.bfloat16),
         in_specs=[anywhere] * 3
-        + [vmem, vmem, pl.BlockSpec(memory_space=pltpu.SMEM), vmem, anywhere, anywhere, anywhere],
+        + [anywhere] * 7,
         out_specs=vmem,
         scratch_shapes=[
             pltpu.VMEM((tok, n_dp * cols), jnp.float32),
@@ -973,10 +1001,14 @@
             pltpu.VMEM((tok, width), jnp.float32),
             pltpu.VMEM((tok, width), jnp.float32),
             pltpu.VMEM((4, tok, width), jnp.float32),
-            dma((6,)),
+            pltpu.VMEM((1, head_size), jnp.float32),
+            pltpu.VMEM((1, head_size), jnp.float32),
+            pltpu.SMEM((count,), jnp.float32),
+            pltpu.VMEM((1, width), jnp.float32),
+            dma((10,)),
             dma((3,)),
             dma((3,)),
-            dma((3, count)),
+            dma((4, count)),
             dma((across,)),
             dma((across, chunks - 1 + ways)),
             dma((across,)),

time: 38.1 us -> 36.8 us (0.966)
  Pallas kernels: 36.8 us -> 35.8 us
    pallas_call x1, Pallas kernels: 36.8 us -> 35.8 us  [split_local(): pl.pallas_call(functools.partial(split_kernel, n, n_dp, n_grp, head_size,...]
where the time goes in v4:
time: 36.8 us; the launch traced here: 36.6 us
  Pallas kernels  35.8 us (97%)
  local copies, waits for them, and re-layouts  0.8 us (2%)
    pallas_call x1, Pallas kernels, split_local(): pl.pallas_call(functools.partial(split_kernel, n, n_dp, n_grp, head_size,...  35.8 us
    unnamed x1, local copies, waits for them, and re-layouts  0.8 us

profile of v4, /device:TPU:30, one launch (start us, length us, event | category | flops | bytes accessed | tf_op | source)
XLA Modules:
  0.0 36.6 jit_solution(5887764337194810174)
XLA Ops:
  0.0 35.8 %shard_map.100 = bf16[1,128,2048]{2,1,0:T(8,128)(2,1)S(1)} custom-call(bf16[1,128,2048]{2,1,0:T(8,128)(2,1)} %q_in.1, bf16[1,128,2048]{2,1,0:T(8,128)(2,1)} %k_in.1, bf16[1,128,2048]{2,1,0:T(8,128)(2,1)} %v_in.1, f32[1,64]{1,0:T(1,128)} %bitcast.3, f32[1,64]{1,0:T(1,128)} %bitcast.4, f32[16]{0:T(128)} %lam_in.1, f32[1,128]{1,0:T(1,128)} %bitcast.5, ...), custom_call_target="tpu_custom_call" | custom-call | tf_op jit(solution)/shard_map/pallas_call | solution.py:981
  35.8 0.8 %copy.12 = bf16[1,128,2048]{2,1,0:T(8,128)(2,1)} copy(bf16[1,128,2048]{2,1,0:T(8,128)(2,1)S(1)} %shard_map.100) | data formatting | bytes 1048576

commit v5 on v4

--- a/solution.py
+++ b/solution.py
@@ -19,13 +19,13 @@
 LAG = 7
 AHEAD = 3
 DEEP = 3
-SPREAD = 4
+PACES = (4, 4, 5, 6)
 BEHIND = 2
 NEAR = 4
-HELP = 5
+HELP = 4
 PROJECT = 10
-SWAP = 2
-PACED = 2
+SWAP = 0
+LATE = 0
 TALKS = ((0, 1), (1, 2), (1, 3), (2, 3))
 MESH = pl.DeviceIdType.MESH
 
@@ -822,12 +822,16 @@
 
     group = GROUP
 
-    def project(g, first, last):
-        step = group * width
-        rows = pl.ds(g * step, step) if isinstance(g, int) else pl.ds(pl.multiple_of(g * step, step), step)
+    def project(g, first, last, parts=((0, GROUP),)):
+        arrived = pl.ds(g * group * width, group * width)
         if cores > 1:
             for xo in range(nx):
-                weight_core_in(xo, g, rows).wait_recv()
+                weight_core_in(xo, g, arrived).wait_recv()
+        for low, high in parts:
+            add_heads(g * group + low, high - low, first, last and high == group)
+
+    def add_heads(low, number, first, last):
+        rows = pl.ds(low * width, number * width)
         block = heads[:, rows]
         for index in range(n_dp):
             term = jnp.dot(block, wfull[index, rows, :], preferred_element_type=jnp.float32)
@@ -899,7 +903,7 @@
             joint_scores(alone + it - GROUP)
 
         for i in range(GROUP):
-            @pl.when((me == 3) & (it == LAG + SPREAD + min(i, PACED)))
+            @pl.when((me == 3) & (it == LAG + PACES[i]))
             def _(i=i):
                 big_to(q_rot, 0, 3, alone + i, 1, 2).start()
                 small_to(0, 1, alone + i, 1, 3).start()
@@ -909,7 +913,7 @@
             upper_third(turned_order(it - LAG))
 
         for g in range(groups - 1):
-            @pl.when(it == g * group + PROJECT + jnp.where(me == 3, 3, jnp.where((me == 1) & (g == 1), 2, 0)))
+            @pl.when(it == g * group + PROJECT + jnp.where(me == 3, LATE, jnp.where((me == 1) & (g == 1), 2, 0)))
             def _(g=g):
                 if g == 0:
                     own_weight.wait()
@@ -917,8 +921,22 @@
 
         return carry
 
-    lax.fori_loop(0, count + LAG, step, 0)
-    project(groups - 1, False, True)
+    steps = count + NEAR
+    lax.fori_loop(0, steps, step, 0)
+
+    @pl.when(me == 3)
+    def _():
+        for h in range(steps - LAG, count - 2):
+            upper_third(h)
+
+    project(groups - 1, False, False, ((0, GROUP - 2),))
+
+    @pl.when(me == 3)
+    def _():
+        for h in range(max(steps - LAG, count - 2), count):
+            upper_third(h)
+
+    add_heads(count - 2, 2, False, True)
 
     whole, most = q_rot.at[:], q_rot.at[0:alone]
     rows = small_out.at[:, 0]

time: 36.8 us -> 35.7 us (0.970)
  Pallas kernels: 35.8 us -> 34.7 us
    pallas_call x1, Pallas kernels: 35.8 us -> 34.7 us  [split_local(): pl.pallas_call(functools.partial(split_kernel, n, n_dp, n_grp, head_size,...]
where the time goes in v5:
time: 35.7 us; the launch traced here: 35.5 us
  Pallas kernels  34.7 us (97%)
  local copies, waits for them, and re-layouts  0.8 us (2%)
    pallas_call x1, Pallas kernels, split_local(): pl.pallas_call(functools.partial(split_kernel, n, n_dp, n_grp, head_size,...  34.7 us
    unnamed x1, local copies, waits for them, and re-layouts  0.8 us

profile of v5, /device:TPU:30, one launch (start us, length us, event | category | flops | bytes accessed | tf_op | source)
XLA Modules:
  0.0 35.5 jit_solution(18359656692765956117)
XLA Ops:
  0.0 34.7 %shard_map.100 = bf16[1,128,2048]{2,1,0:T(8,128)(2,1)S(1)} custom-call(bf16[1,128,2048]{2,1,0:T(8,128)(2,1)} %q_in.1, bf16[1,128,2048]{2,1,0:T(8,128)(2,1)} %k_in.1, bf16[1,128,2048]{2,1,0:T(8,128)(2,1)} %v_in.1, f32[1,64]{1,0:T(1,128)} %bitcast.3, f32[1,64]{1,0:T(1,128)} %bitcast.4, f32[16]{0:T(128)} %lam_in.1, f32[1,128]{1,0:T(1,128)} %bitcast.5, ...), custom_call_target="tpu_custom_call" | custom-call | tf_op jit(solution)/shard_map/pallas_call | solution.py:999
  34.7 0.8 %copy.12 = bf16[1,128,2048]{2,1,0:T(8,128)(2,1)} copy(bf16[1,128,2048]{2,1,0:T(8,128)(2,1)S(1)} %shard_map.100) | data formatting | bytes 1048576

commit v6 on v5

--- a/solution.py
+++ b/solution.py
@@ -19,7 +19,7 @@
 LAG = 7
 AHEAD = 3
 DEEP = 3
-PACES = (4, 4, 5, 6)
+PACES = (4, 4, 6, 6)
 BEHIND = 2
 NEAR = 4
 HELP = 4

time: 35.7 us -> 35.5 us (level)
  no operation moved by 1% of the time
where the time goes in v6:
time: 35.5 us; the launch traced here: 35.2 us
  Pallas kernels  34.4 us (97%)
  local copies, waits for them, and re-layouts  0.8 us (2%)
    pallas_call x1, Pallas kernels, split_local(): pl.pallas_call(functools.partial(split_kernel, n, n_dp, n_grp, head_size,...  34.4 us
    unnamed x1, local copies, waits for them, and re-layouts  0.8 us

profile of v6, /device:TPU:30, one launch (start us, length us, event | category | flops | bytes accessed | tf_op | source)
XLA Modules:
  0.0 35.2 jit_solution(2615208153211669579)
XLA Ops:
  0.0 34.4 %shard_map.100 = bf16[1,128,2048]{2,1,0:T(8,128)(2,1)S(1)} custom-call(bf16[1,128,2048]{2,1,0:T(8,128)(2,1)} %q_in.1, bf16[1,128,2048]{2,1,0:T(8,128)(2,1)} %k_in.1, bf16[1,128,2048]{2,1,0:T(8,128)(2,1)} %v_in.1, f32[1,64]{1,0:T(1,128)} %bitcast.3, f32[1,64]{1,0:T(1,128)} %bitcast.4, f32[16]{0:T(128)} %lam_in.1, f32[1,128]{1,0:T(1,128)} %bitcast.5, ...), custom_call_target="tpu_custom_call" | custom-call | tf_op jit(solution)/shard_map/pallas_call | solution.py:999
  34.4 0.8 %copy.12 = bf16[1,128,2048]{2,1,0:T(8,128)(2,1)} copy(bf16[1,128,2048]{2,1,0:T(8,128)(2,1)S(1)} %shard_map.100) | data formatting | bytes 1048576
